TPU v7x, 128 devices: a whole 4x4x4 slice. The times are simulated.
128 devices in a mesh: rep: 2 (over x_hi), fs: 16 (over y, x_lo, core), tp: 4 (over z).
Axes of the slice: x: 4 (x_hi: 2, x_lo: 2; x = x_hi * 2 + x_lo), y: 4, z: 4, core: 2. Of those that a mesh axis runs over, the one named last changes fastest.
Arguments:
- acts: bfloat16 [8192, 2048], P(('rep', 'fs'), 'tp'), may hold values from -6 to 6
- cotangent: bfloat16 [8192, 2048], P(('rep', 'fs'), 'tp'), may hold values from -8 to 8
- pre_act: bfloat16 [8192, 4096], P(('rep', 'fs'), 'tp'), may hold values from -6 to 6
- up_store: float32 [2048, 4096], P('fs', 'tp'), may hold values from -0.125 to 0.125
- up_scale: float32 [4096], P('tp'), may hold values from 0.5 to 2
- down_store: float32 [4096, 2048], P('tp', 'fs'), may hold values from -0.09375 to 0.09375
- down_scale: float32 [2048], replicated, may hold values from 0.5 to 2
Outputs:
- grad_input: bfloat16 [8192, 2048], P(('rep', 'fs'), 'tp')
- grad_up: float32 [2048, 4096], P('fs', 'tp')
- grad_down: float32 [4096, 2048], P('tp', 'fs')
All inputs are finite; a program needn't handle non-finite values.
Results may differ from a plain program's by a relative error of at most 0.007.
Values may be sent and summed in bfloat16 or wider, within the bound.
A program may use at most 128 MiB of HBM per device.

v0:
```python
import math

import jax
import jax.numpy as jnp
from jax import lax
from jax.sharding import PartitionSpec as P


def sent_together(arrays, axis, dim, along):
    ends, at = ([], 0)
    for a in arrays[:-1]:
        at += a.shape[along]
        ends.append(at)
    both = jnp.concatenate(arrays, axis=along)
    return tuple(jnp.split(lax.all_gather(both, axis, axis=dim, tiled=True), ends, axis=along))


def copy_for_each(x, axis):
    count = lax.axis_size(axis)
    return lax.all_to_all(jnp.broadcast_to(x[None], (count, *x.shape)), axis, 0, 0, tiled=True)


def of_everyone(x, axis):
    return copy_for_each(x, axis).sum(axis=0)


def in_blocks(x, dim, count):
    lengths = x.shape
    tiles = x.reshape(*lengths[:dim], count, lengths[dim] // count, *lengths[dim + 1 :])
    return jnp.moveaxis(tiles, dim, 0)


def summed_on_arrival(x, axis, dim):
    tiles = in_blocks(x, dim, lax.axis_size(axis))
    arrived = lax.all_to_all(tiles, axis, split_axis=0, concat_axis=0, tiled=True)
    return arrived.sum(axis=0)


def contract_last(left, right):
    return lax.dot_general(
        left, right, (((1,), (1,)), ((), ())), preferred_element_type=jnp.float32
    )


def contract_first(left, right):
    return lax.dot_general(
        left, right, (((0,), (0,)), ((), ())), preferred_element_type=jnp.float32
    )


def body(acts, cotangent, pre_act, up_store, up_scale, down_store, down_scale):
    tok_rows = acts.shape[0]
    norm_factor = 1.0 / math.sqrt(tok_rows * lax.axis_size("fs") * lax.axis_size("rep"))
    full_acts, full_cot = sent_together((acts, cotangent), "tp", 1, 0)
    scaled = (full_cot.astype(jnp.float32) * down_scale[None, :]).astype(jnp.bfloat16)
    down_bf = down_store.astype(jnp.bfloat16)
    up_bf = up_store.astype(jnp.bfloat16)
    d_act = contract_last(scaled, lax.all_gather(down_bf, "fs", axis=1, tiled=True))
    positive = jnp.maximum(pre_act.astype(jnp.float32), 0.0)
    act = (positive * positive).astype(jnp.bfloat16)
    d_pre = (2.0 * positive * d_act * up_scale[None, :]).astype(jnp.bfloat16)
    acts_cols, scaled_cols = (
        lax.all_to_all(full_acts, "fs", split_axis=1, concat_axis=0, tiled=True),
        lax.all_to_all(scaled, "fs", split_axis=1, concat_axis=0, tiled=True),
    )
    act_group, dpre_group = sent_together((act, d_pre), "fs", 0, 1)
    grad_down = contract_first(act_group, scaled_cols) * norm_factor
    grad_up = contract_first(acts_cols, dpre_group) * norm_factor
    grad_down = of_everyone(grad_down, "rep")
    partial_value = contract_last(d_pre, lax.all_gather(up_bf, "fs", axis=0, tiled=True))
    grad_input = summed_on_arrival(partial_value, "tp", 1).astype(jnp.bfloat16)
    grad_up = of_everyone(grad_up, "rep")
    return (grad_input, grad_up, grad_down)


def solution(mesh):
    return jax.shard_map(
        body,
        mesh=mesh,
        in_specs=(
            P(("rep", "fs"), "tp"),
            P(("rep", "fs"), "tp"),
            P(("rep", "fs"), "tp"),
            P("fs", "tp"),
            P("tp"),
            P("tp", "fs"),
            P(),
        ),
        out_specs=(P(("rep", "fs"), "tp"), P("fs", "tp"), P("tp", "fs")),
        check_vma=False,
    )
```

profile of v0, /device:TPU:0, one launch (start us, length us, event | category | flops | bytes accessed | tf_op | source)
XLA Modules:
  0.0 299.9 jit_solution(1062282889312166181)
XLA Ops:
  7.2 1.1 copy.20
  10.4 1.8 convert_element_type.27
  12.2 1.8 convert_element_type.29
  14.2 29.7 %all-gather.5.cloned.1.call-done = bf16[512,2048]{0,1:T(8,128)(2,1)} async-done(((bf16[512,512]{0,1:T(8,128)(2,1)}), bf16[512,2048]{0,1:T(8,128)(2,1)}) %all-gather.5.cloned.1.call-update) | async-done | bytes 2097168 | tf_op jit(solution)/shard_map/all_gather | solution.py:15
  44.0 2.6 multiply_convert_fusion
  46.6 44.5 %all-gather.7.cloned.1.call-done = bf16[1024,2048]{1,0:T(8,128)(2,1)} async-done(((bf16[1024,128]{1,0:T(8,128)(2,1)}), bf16[1024,2048]{1,0:T(8,128)(2,1)}) %all-gather.7.cloned.1.call-update) | async-done | bytes 4194320 | tf_op jit(solution)/shard_map/all_gather | solution.py:58
  91.1 3.9 %fusion.5 = bf16[256,1024]{1,0:T(8,128)(2,1)S(1)} fusion(bf16[256,2048]{0,1:T(8,128)(2,1)} %multiply_convert_fusion, bf16[1024,2048]{1,0:T(8,128)(2,1)} %all-gather.7.cloned.1.call-done, bf16[256,1024]{1,0:T(8,128)(2,1)S(1)} %copy-done.1, f32[1024]{0:T(1024)S(1)} %copy-done.3), kind=kOutput, calls=%fused_computation.8 | convolution fusion | flops 1075314688 | bytes 6295552 | tf_op jit(solution)/shard_map/dot_general | solution.py:40
  96.6 28.0 %all_to_all.53 = bf16[256,16,128]{0,2,1:T(8,128)(2,1)S(1)} all-to-all(bf16[256,16,128]{0,2,1:T(8,128)(2,1)S(1)} %bitcast.22), channel_id=1, replica_groups=mesh['rep'=2,'fs'=16,'tp'=4] {'fs'}, dimensions={1} | all-to-all | bytes 2097152 | tf_op jit(solution)/shard_map/all_to_all | solution.py:63
  124.6 3.7 %all-to-all-start.3 = ((bf16[256,16,128]{0,2,1:T(8,128)(2,1)}), bf16[256,16,128]{0,2,1:T(8,128)(2,1)S(1)}, u32[]{:S(2)}, u32[]{:S(2)}) async-start(bf16[256,16,128]{0,2,1:T(8,128)(2,1)} %bitcast.4), calls=%async_computation.3 | async-start | bytes 2097152 | tf_op jit(solution)/shard_map/all_to_all | solution.py:64
  128.3 22.2 %all-gather.9.cloned.1.call-done = bf16[2048,1024]{1,0:T(8,128)(2,1)} async-done(((bf16[128,1024]{1,0:T(8,128)(2,1)}), bf16[2048,1024]{1,0:T(8,128)(2,1)}) %all-gather.9.cloned.1.call-update) | async-done | bytes 4194320 | tf_op jit(solution)/shard_map/all_gather | solution.py:70
  150.5 3.5 %fusion.12 = f32[256,2048]{1,0:T(8,128)S(1)} fusion(bf16[256,1024]{1,0:T(8,128)(2,1)S(1)} %fusion.5, bf16[2048,1024]{1,0:T(8,128)(2,1)} %all-gather.9.cloned.1.call-done), kind=kOutput, calls=%fused_computation.15 | convolution fusion | flops 1073741824 | bytes 6815744 | tf_op jit(solution)/shard_map/dot_general | solution.py:40
  154.0 1.5 copy.26
  156.5 4.4 %all-to-all-start = ((f32[4,256,512]{2,1,0:T(8,128)}), f32[4,256,512]{2,1,0:T(8,128)S(1)}, u32[]{:S(2)}, u32[]{:S(2)}) async-start(f32[4,256,512]{2,1,0:T(8,128)} %bitcast.19), calls=%async_computation | async-start | bytes 4194304 | tf_op jit(solution)/shard_map/all_to_all | solution.py:35
  160.9 1.3 copy.22
  162.2 2.3 copy.23
  164.5 79.5 %all-gather.11.cloned.1.call-done = bf16[4096,2048]{1,0:T(8,128)(2,1)} async-done(((bf16[256,2048]{1,0:T(8,128)(2,1)}), bf16[4096,2048]{1,0:T(8,128)(2,1)}) %all-gather.11.cloned.1.call-update) | async-done | bytes 16777232 | tf_op jit(solution)/shard_map/all_gather | solution.py:15
  244.1 5.0 %fusion.6 = f32[128,1024]{1,0:T(8,128)S(1)} fusion(bf16[4096,128]{1,0:T(8,128)(2,1)} %bitcast.25, bf16[4096,2048]{1,0:T(8,128)(2,1)} %all-gather.11.cloned.1.call-done), kind=kOutput, calls=%fused_computation.9 | convolution fusion | flops 1073872896 | bytes 9961472 | tf_op jit(solution)/shard_map/dot_general | solution.py:46
  250.2 4.2 %all-to-all-start.2 = ((f32[2,128,1024]{2,1,0:T(8,128)}), f32[2,128,1024]{2,1,0:T(8,128)S(1)}, u32[]{:S(2)}, u32[]{:S(2)}) async-start(f32[2,128,1024]{2,1,0:T(8,128)} %broadcast_in_dim.4), calls=%async_computation.2 | async-start | bytes 2097152 | tf_op jit(solution)/shard_map/all_to_all | solution.py:20
  254.4 6.8 %fusion.9 = f32[1024,128]{1,0:T(8,128)} fusion(bf16[4096,128]{1,0:T(8,128)(2,1)} %bitcast.24, bf16[4096,2048]{1,0:T(8,128)(2,1)} %all-gather.11.cloned.1.call-done), kind=kOutput, calls=%fused_computation.10 | convolution fusion | flops 1073872896 | bytes 9961472 | tf_op jit(solution)/shard_map/dot_general | solution.py:46
  261.2 8.7 %all-to-all-done.2 = f32[2,128,1024]{2,1,0:T(8,128)S(1)} async-done(((f32[2,128,1024]{2,1,0:T(8,128)}), f32[2,128,1024]{2,1,0:T(8,128)S(1)}, u32[]{:S(2)}, u32[]{:S(2)}) %all-to-all-start.2) | async-done | bytes 1048608 | tf_op jit(solution)/shard_map/all_to_all | solution.py:20
  269.9 2.1 broadcast_in_dim.5
  272.1 4.4 %all-to-all-start.4 = ((f32[2,1024,128]{2,1,0:T(8,128)}), f32[2,1024,128]{2,1,0:T(8,128)}, u32[]{:S(2)}, u32[]{:S(2)}) async-start(f32[2,1024,128]{2,1,0:T(8,128)} %broadcast_in_dim.5), calls=%async_computation.4 | async-start | bytes 2097152 | tf_op jit(solution)/shard_map/all_to_all | solution.py:20
  278.3 12.9 %all-to-all-done.4 = f32[2,1024,128]{2,1,0:T(8,128)} async-done(((f32[2,1024,128]{2,1,0:T(8,128)}), f32[2,1024,128]{2,1,0:T(8,128)}, u32[]{:S(2)}, u32[]{:S(2)}) %all-to-all-start.4) | async-done | bytes 1048608 | tf_op jit(solution)/shard_map/all_to_all | solution.py:20
  291.2 2.1 reduce_sum.29
  (27 shorter events, 7.8 us)
Async XLA Ops:
  7.2 6.9 %copy-start.1 = (bf16[256,1024]{1,0:T(8,128)(2,1)S(1)}, bf16[256,1024]{1,0:T(8,128)(2,1)}, u32[]{:S(2)}) copy-start(bf16[256,1024]{1,0:T(8,128)(2,1)} %param.9) | copy-start | bytes 1572868
  7.2 36.8 %copy-start.2 = (f32[2048]{0:T(1024)S(1)}, f32[2048]{0:T(1024)}, u32[]{:S(2)}) copy-start(f32[2048]{0:T(1024)} %param.13) | copy-start | bytes 24580
  7.2 83.9 %copy-start.3 = (f32[1024]{0:T(1024)S(1)}, f32[1024]{0:T(1024)}, u32[]{:S(2)}) copy-start(f32[1024]{0:T(1024)} %param.11) | copy-start | bytes 12292
  7.2 36.8 %all-gather.5.cloned.1.call-start = ((), (), s32[]{:S(2)}) async-start(), calls=%async_computation.5 | async-start | bytes 2621440 | tf_op jit(solution)/shard_map/all_gather | solution.py:15
  10.3 80.7 %all-gather.7.cloned.1.call-start = ((), (), s32[]{:S(2)}) async-start(), calls=%async_computation.6 | async-start | bytes 4456448 | tf_op jit(solution)/shard_map/all_gather | solution.py:58
  12.2 138.3 %all-gather.9.cloned.1.call-start = ((), (), s32[]{:S(2)}) async-start(), calls=%async_computation.7 | async-start | bytes 4456448 | tf_op jit(solution)/shard_map/all_gather | solution.py:70
  14.0 230.0 %all-gather.11.cloned.1.call-start = ((), (), s32[]{:S(2)}) async-start(), calls=%async_computation.8 | async-start | bytes 17825792 | tf_op jit(solution)/shard_map/all_gather | solution.py:15
  95.0 1.6 slice-start
  124.6 30.9 %all-to-all-start.3 = ((bf16[256,16,128]{0,2,1:T(8,128)(2,1)}), bf16[256,16,128]{0,2,1:T(8,128)(2,1)S(1)}, u32[]{:S(2)}, u32[]{:S(2)}) async-start(bf16[256,16,128]{0,2,1:T(8,128)(2,1)} %bitcast.4), calls=%async_computation.3 | async-start | bytes 2097152 | tf_op jit(solution)/shard_map/all_to_all | solution.py:64
  155.5 1.0 copy-start
  156.5 92.6 %all-to-all-start = ((f32[4,256,512]{2,1,0:T(8,128)}), f32[4,256,512]{2,1,0:T(8,128)S(1)}, u32[]{:S(2)}, u32[]{:S(2)}) async-start(f32[4,256,512]{2,1,0:T(8,128)} %bitcast.19), calls=%async_computation | async-start | bytes 4194304 | tf_op jit(solution)/shard_map/all_to_all | solution.py:35
  250.2 19.8 %all-to-all-start.2 = ((f32[2,128,1024]{2,1,0:T(8,128)}), f32[2,128,1024]{2,1,0:T(8,128)S(1)}, u32[]{:S(2)}, u32[]{:S(2)}) async-start(f32[2,128,1024]{2,1,0:T(8,128)} %broadcast_in_dim.4), calls=%async_computation.2 | async-start | bytes 2097152 | tf_op jit(solution)/shard_map/all_to_all | solution.py:20
  272.1 19.1 %all-to-all-start.4 = ((f32[2,1024,128]{2,1,0:T(8,128)}), f32[2,1024,128]{2,1,0:T(8,128)}, u32[]{:S(2)}, u32[]{:S(2)}) async-start(f32[2,1024,128]{2,1,0:T(8,128)} %broadcast_in_dim.5), calls=%async_computation.4 | async-start | bytes 2097152 | tf_op jit(solution)/shard_map/all_to_all | solution.py:20
Sparse Core Ops, SparseCore 0:
  10.4 33.4 all-gather.4
  46.2 44.8 all-gather.6
  93.3 57.1 all-gather.8
  152.1 91.9 all-gather.10
where the time goes:
time: 301 us; the launch traced here: 300 us
  waiting for transfers between devices  198 us (66%)
  blocking collectives  28 us (9%)
  matrix products  19.1 us (6%)
  starting transfers between devices  16.9 us (6%)
  between operations  13.9 us (5%)
  other arithmetic  12.2 us (4%)
  local copies, waits for them, and re-layouts  12.1 us (4%)
    all_gather x2, waiting for transfers between devices, sent_together(): lax.all_gather(both, axis, axis=dim, tiled=True)  109 us
    all_gather x1, waiting for transfers between devices, body(): lax.all_gather(down_bf, 'fs', axis=1, tiled=True)  44.5 us
    all_to_all x1, blocking collectives, body(): lax.all_to_all(full_acts, 'fs', split_axis=1, concat_axis=0, tiled=True)  28 us
    all_gather x1, waiting for transfers between devices, body(): lax.all_gather(up_bf, 'fs', axis=0, tiled=True)  22.2 us
    all_to_all x2, waiting for transfers between devices, copy_for_each(): lax.all_to_all(jnp.broadcast_to(x[None], (count, *x.shape)), axis, 0, 0,...  21.6 us
    dot_general x2, matrix products, contract_first(): lax.dot_general(left, right, (((0,), (0,)), ((), ())), preferred_element_...  11.8 us
    all_to_all x2, starting transfers between devices, copy_for_each(): lax.all_to_all(jnp.broadcast_to(x[None], (count, *x.shape)), axis, 0, 0,...  8.65 us
    dot_general x2, matrix products, contract_last(): lax.dot_general(left, right, (((1,), (1,)), ((), ())), preferred_element_...  7.37 us
  transfers between devices with their start and end apart: 8, of which 6 were waited for; matrix products, arithmetic and copies ran while one was open for 11% of the time, Pallas kernels for 0%

commit v1 on v0

v1 whole, which is shorter than its diff:
```python
import math

import jax
import jax.numpy as jnp
from jax import lax
from jax.experimental import pallas as pl
from jax.experimental.pallas import tpu as pltpu
from jax.sharding import PartitionSpec as P

BF = jnp.bfloat16
F32 = jnp.float32
MESH = pl.DeviceIdType.MESH
COPIES = 96


def nt(a, b):
    return lax.dot_general(a, b, (((1,), (1,)), ((), ())), preferred_element_type=F32)


def nn(a, b):
    return lax.dot_general(a, b, (((1,), (0,)), ((), ())), preferred_element_type=F32)


def kernel(
    norm, cot, acts, pre, up, ups, down, dsc,
    gi_out, gu_out, gd_out,
    loc_s, loc_a, xs, xa, pre_r, act_t, wd, wu, da, dr, dpre,
    pd, rxd, sd, y2pd, y2md, ypd, ymd, fd, rrd,
    pu, rxu, su, y2pu, y2mu, ypu, ymu, fu, rru,
    gi, z2p, z2m, zp, zm, fz, rd,
    ssem, rsem,
):
    r, f, z = (lax.axis_index(n) for n in ("rep", "fs", "tp"))
    y = lax.div(f, 4)
    xl = lax.rem(lax.div(f, 2), 2)
    c = lax.rem(f, 2)
    x = r * 2 + xl
    oc, ox = 1 - c, 1 - xl

    def dev(dx=0, dy=0, dz=0, core=None):
        nx, ny, nz = (lax.rem(a + d + 4, 4) for a, d in ((x, dx), (y, dy), (z, dz)))
        core = c if core is None else core
        return {
            "rep": lax.div(nx, 2),
            "fs": ny * 4 + lax.rem(nx, 2) * 2 + core,
            "tp": nz,
        }

    def at(a, d):
        return lax.rem(a + d + 4, 4)

    barrier = pltpu.get_barrier_semaphore()
    peers = [dev(dz=d, core=k) for d in (1, -1) for k in (c, oc)]
    peers += [dev(dy=1), dev(dy=-1), dev(dx=1), dev(dx=-1), dev(dx=2), dev(core=oc)]
    for p in peers:
        pl.semaphore_signal(barrier, inc=1, device_id=p, device_id_type=MESH)

    started = []

    def send(src, dst, to):
        k = len(started)
        copy = pltpu.make_async_remote_copy(
            src_ref=src, dst_ref=dst, send_sem=ssem.at[k], recv_sem=rsem.at[k],
            device_id=to, device_id_type=MESH,
        )
        copy.start()
        started.append(copy)
        return copy

    scale = dsc[:, pl.ds(pl.multiple_of(z * 512, 512), 512)]
    scaled = (cot[...].astype(F32) * scale).astype(BF)
    for k in range(2):
        for j in range(2):
            lanes = slice(j * 256 + k * 128, j * 256 + k * 128 + 128)
            loc_s[k, :, j * 128:(j + 1) * 128] = scaled[:, lanes]
            loc_a[k, :, j * 128:(j + 1) * 128] = acts[:, lanes]
    wd[y, xl] = down[...].astype(BF)
    wu[y, xl] = up[...].astype(BF)
    xs[z, 0:256, :] = loc_s[c]
    xa[z, 0:256, :] = loc_a[c]
    pl.semaphore_wait(barrier, len(peers))

    own, other = pl.ds(0, 256), pl.ds(256, 256)

    def z_send(loc, full):
        out = []
        for d in (1, -1):
            out.append(send(loc.at[c], full.at[z, own, :], dev(dz=d)))
            out.append(send(loc.at[oc], full.at[z, other, :], dev(dz=d, core=oc)))
        out.append(send(loc.at[oc], full.at[z, other, :], dev(core=oc)))
        return out

    def z_forward(full, first):
        first[0].wait_recv()
        a = send(full.at[at(z, -1), own, :], full.at[at(z, -1), own, :], dev(dz=1))
        first[3].wait_recv()
        b = send(full.at[at(z, 1), other, :], full.at[at(z, 1), other, :], dev(dz=-1))
        return [first[1], first[2], first[4], a, b]

    def half(ref, k, xx, h):
        rows = ref.shape[2] // 2
        return ref.at[k, xx, pl.ds(h * rows, rows), :]

    def x_send(w, k, h):
        return send(half(w, k, xl, h), half(w, k, xl, h), dev(dx=1 - 2 * h))

    def w_first(w):
        return [send(w.at[y, xl], w.at[y, xl], dev(dy=d)) for d in (1, -1)]

    def w_second(w, first):
        fwd = []
        xsend = []
        for h, d in ((0, 1), (1, -1)):
            first[h].wait_recv()
            k = at(y, -d)
            fwd.append(send(half(w, k, xl, h), half(w, k, xl, h), dev(dy=d)))
            xsend += [x_send(w, k, 0), x_send(w, k, 1)]
        return fwd, xsend

    def w_third(w, fwd):
        xsend = []
        for h in range(2):
            fwd[h].wait_recv()
            xsend.append(x_send(w, at(y, 2), h))
        return xsend

    def wait_recv(copies):
        for k in copies:
            k.wait_recv()

    s1 = z_send(loc_s, xs)
    wd1 = w_first(wd)
    wdx = [x_send(wd, y, 0), x_send(wd, y, 1)]
    pre1 = send(pre, pre_r, dev(core=oc))
    s2 = z_forward(xs, s1)
    a1 = z_send(loc_a, xa)
    wd2, more = w_second(wd, wd1)
    wdx += more
    wu1 = w_first(wu)
    wux = [x_send(wu, y, 0), x_send(wu, y, 1)]

    def relu_sq(v):
        p = jnp.maximum(v.astype(F32), 0.0)
        return (p * p).astype(BF)

    act_t[:, 0:256] = relu_sq(pre[...]).T
    pre1.wait_recv()
    act_t[:, 256:512] = relu_sq(pre_r[...]).T
    wait_recv(s2)
    wdx += w_third(wd, wd2)

    for k in range(4):
        part = nn(act_t[...], xs[k])
        for j in range(2):
            pd[k, j] = part[:, j * 128:(j + 1) * 128].astype(BF)
    order = (2, 1, -1, 0)

    def scatter_x(part, rx):
        out = {}
        for d in order:
            k = at(y, d)
            out[d] = []
            for h in range(2):
                rows = part.shape[2] // 2
                out[d].append(
                    send(half(part, k, ox, h), rx.at[k, pl.ds(h * rows, rows), :], dev(dx=1 - 2 * h))
                )
        return out

    dx = scatter_x(pd, rxd)
    a2 = z_forward(xa, a1)
    wu2, more = w_second(wu, wu1)
    wux += more

    wait_recv(wdx)
    dax = []
    for h in range(2):
        total = None
        for k in range(4):
            w = jnp.concatenate([wd[k, 0], wd[k, 1]], axis=1)
            term = nt(xs[k, h * 256:(h + 1) * 256, :], w)
            total = term if total is None else total + term
        da[h] = total
        dax.append(send(da.at[h], dr.at[1 - h], dev(core=oc)))
    wux += w_third(wu, wu2)
    wait_recv(a2)
    for h in (1, 0):
        dax[1 - h].wait_recv()
        src = pre if h == 0 else pre_r
        pos = jnp.maximum(src[...].astype(F32), 0.0)
        dpre[h * 256:(h + 1) * 256, :] = (2.0 * pos * (da[h] + dr[h]) * ups[...]).astype(BF)

    for k in range(4):
        part = nn(xa[k].T, dpre[...])
        for j in range(2):
            pu[k, j] = part[j * 128:(j + 1) * 128, :].astype(BF)
    ux = scatter_x(pu, rxu)

    def add(a, b):
        return a.astype(F32) + b.astype(F32)

    def sum_x(part, rx, s, xcopies, d):
        wait_recv(xcopies[d])
        k = at(y, d)
        s[k] = add(part[k, xl], rx[k]).astype(BF)

    def ring_far(s, me, r2p, r2m, nxt, prv):
        n = s.shape[1] // 2
        k = at(me, 2)
        return [
            send(s.at[k, pl.ds(0, n), :], r2p, nxt),
            send(s.at[k, pl.ds(n, n), :], r2m, prv),
        ]

    def ring_near(s, me, far, r2p, r2m, rp, rm, nxt, prv):
        n = s.shape[1] // 2
        out = []
        kp, km = at(me, 1), at(me, -1)
        out.append(send(s.at[kp, pl.ds(n, n), :], rp.at[pl.ds(n, n), :], nxt))
        out.append(send(s.at[km, pl.ds(0, n), :], rm.at[pl.ds(0, n), :], prv))
        far[0].wait_recv()
        s[kp, 0:n, :] = add(s[kp, 0:n, :], r2p[...]).astype(BF)
        out.append(send(s.at[kp, pl.ds(0, n), :], rp.at[pl.ds(0, n), :], nxt))
        far[1].wait_recv()
        s[km, n:, :] = add(s[km, n:, :], r2m[...]).astype(BF)
        out.append(send(s.at[km, pl.ds(n, n), :], rm.at[pl.ds(n, n), :], prv))
        return out

    ypn, ymn, zpn, zmn = dev(dy=1), dev(dy=-1), dev(dz=1), dev(dz=-1)
    sum_x(pd, rxd, sd, dx, 2)
    dfar = ring_far(sd, y, y2pd, y2md, ypn, ymn)
    sum_x(pd, rxd, sd, dx, 1)
    sum_x(pd, rxd, sd, dx, -1)

    wait_recv(wux)
    for k in range(4):
        w = wu[k].reshape(256, 1024)
        gi[k] = nt(dpre[...], w).astype(BF)
    zfar = ring_far(gi, z, z2p, z2m, zpn, zmn)
    dnear = ring_near(sd, y, dfar, y2pd, y2md, ypd, ymd, ypn, ymn)
    sum_x(pd, rxd, sd, dx, 0)
    znear = ring_near(gi, z, zfar, z2p, z2m, zp, zm, zpn, zmn)

    sum_x(pu, rxu, su, ux, 2)
    ufar = ring_far(su, y, y2pu, y2mu, ypn, ymn)
    sum_x(pu, rxu, su, ux, 1)
    sum_x(pu, rxu, su, ux, -1)

    wait_recv(dnear)
    fd[...] = (add(sd[y], ypd[...]) + ymd[...].astype(F32)).astype(BF)
    drep = send(fd, rrd, dev(dx=2))

    unear = ring_near(su, y, ufar, y2pu, y2mu, ypu, ymu, ypn, ymn)
    sum_x(pu, rxu, su, ux, 0)

    wait_recv(znear)
    fz[...] = (add(gi[z], zp[...]) + zm[...].astype(F32)).astype(BF)
    dz = send(fz.at[other, :], rd, dev(core=oc))

    wait_recv(unear)
    fu[...] = (add(su[y], ypu[...]) + ymu[...].astype(F32)).astype(BF)
    urep = send(fu, rru, dev(dx=2))

    dz.wait_recv()
    for j in range(2):
        lanes = pl.ds(pl.multiple_of(j * 256 + c * 128, 128), 128)
        gi_out[:, lanes] = fz[0:256, j * 128:(j + 1) * 128]
        lanes = pl.ds(pl.multiple_of(j * 256 + oc * 128, 128), 128)
        gi_out[:, lanes] = rd[:, j * 128:(j + 1) * 128]
    drep.wait_recv()
    gd_out[...] = add(fd[...], rrd[...]) * norm
    urep.wait_recv()
    gu_out[...] = add(fu[...], rru[...]) * norm
    for copy in started:
        copy.wait_send()


def body(acts, cotangent, pre_act, up_store, up_scale, down_store, down_scale):
    tokens = acts.shape[0] * lax.axis_size("fs") * lax.axis_size("rep")
    norm = 1.0 / math.sqrt(tokens)

    def vm(*shape, dtype=BF):
        return pltpu.VMEM(shape, dtype)

    def grad_bufs(a, b):
        h = a // 2
        return [
            vm(4, 2, a, b), vm(4, a, b), vm(4, a, b), vm(h, b), vm(h, b),
            vm(a, b), vm(a, b), vm(a, b), vm(a, b),
        ]

    spec = pl.BlockSpec(memory_space=pltpu.VMEM)

    def call(*args):
        return kernel(norm, *args)

    return pl.pallas_call(
        call,
        name="ffn_backward",
        out_shape=(
            jax.ShapeDtypeStruct((256, 512), BF),
            jax.ShapeDtypeStruct((128, 1024), F32),
            jax.ShapeDtypeStruct((1024, 128), F32),
        ),
        in_specs=[spec] * 7,
        out_specs=(spec,) * 3,
        scratch_shapes=[
            vm(2, 256, 256), vm(2, 256, 256), vm(4, 512, 256), vm(4, 512, 256),
            vm(256, 1024), vm(1024, 512), vm(4, 2, 1024, 128), vm(4, 2, 128, 1024),
            vm(2, 256, 1024, dtype=F32), vm(2, 256, 1024, dtype=F32), vm(512, 1024),
            *grad_bufs(1024, 128),
            *grad_bufs(128, 1024),
            vm(4, 512, 256), vm(256, 256), vm(256, 256), vm(512, 256), vm(512, 256),
            vm(512, 256), vm(256, 256),
            pltpu.SemaphoreType.DMA((COPIES,)),
            pltpu.SemaphoreType.DMA((COPIES,)),
        ],
        compiler_params=pltpu.CompilerParams(
            collective_id=0, has_side_effects=True, vmem_limit_bytes=56 * 1024 * 1024
        ),
    )(
        cotangent, acts, pre_act, up_store, up_scale.reshape(1, -1),
        down_store, down_scale.reshape(1, -1),
    )


def solution(mesh):
    return jax.shard_map(
        body,
        mesh=mesh,
        in_specs=(
            P(("rep", "fs"), "tp"),
            P(("rep", "fs"), "tp"),
            P(("rep", "fs"), "tp"),
            P("fs", "tp"),
            P("tp"),
            P("tp", "fs"),
            P(),
        ),
        out_specs=(P(("rep", "fs"), "tp"), P("fs", "tp"), P("tp", "fs")),
        check_vma=False,
    )
```

time: 301 us -> 80.7 us (0.27)
  waiting for transfers between devices: 198 us -> 0 us
  Pallas kernels: 0 us -> 75.8 us
  blocking collectives: 28 us -> 0 us
  matrix products: 19.1 us -> 0 us
  starting transfers between devices: 16.9 us -> 0 us
  between operations: 13.9 us -> 0.65 us
  other arithmetic: 12.2 us -> 0 us
  local copies, waits for them, and re-layouts: 12.1 us -> 3.75 us
    all_gather x4 -> x0, waiting for transfers between devices: 176 us -> none  [the longest x2 109 us: sent_together(): lax.all_gather(both, axis, axis=dim, tiled=True)]
    pallas_call x0 -> x1, Pallas kernels: none -> 75.8 us  [body(): pl.pallas_call(call, name='ffn_backward', out_shape=(jax.ShapeDtypeStruct...]
    all_to_all x1 -> x0, blocking collectives: 28 us -> none  [body(): lax.all_to_all(full_acts, 'fs', split_axis=1, concat_axis=0, tiled=True)]
    all_to_all x4 -> x0, waiting for transfers between devices: 21.6 us -> none  [the longest x2 21.6 us: copy_for_each(): lax.all_to_all(jnp.broadcast_to(x[None], (count, *x.shape)), axis, 0, 0,...]
    dot_general x4 -> x0, matrix products: 19.1 us -> none  [the longest x2 11.8 us: contract_first(): lax.dot_general(left, right, (((0,), (0,)), ((), ())), preferred_element_...]
    all_to_all x4 -> x0, starting transfers between devices: 16.7 us -> none  [the longest x2 8.65 us: copy_for_each(): lax.all_to_all(jnp.broadcast_to(x[None], (count, *x.shape)), axis, 0, 0,...]
    convert_element_type x4 -> x0, other arithmetic: 6.28 us -> none  [the longest x1 2.6 us: body(): (full_cot.astype(jnp.float32) * down_scale[None, :]).astype(jnp.bfloat16)]
    reduce_sum x3 -> x0, other arithmetic: 3.99 us -> none  [the longest x2 3.03 us: of_everyone(): return copy_for_each(x, axis).sum(axis=0)]
  transfers between devices with their start and end apart: 8 -> 0, of which waited for: 6 -> 0; matrix products, arithmetic and copies ran while one was open for 11% -> 0% of each run, Pallas kernels for 0% -> 0%
where the time goes in v1:
time: 80.7 us; the launch traced here: 80.2 us
  Pallas kernels  75.8 us (94%)
  local copies, waits for them, and re-layouts  3.75 us (5%)
    pallas_call x1, Pallas kernels, body(): pl.pallas_call(call, name='ffn_backward', out_shape=(jax.ShapeDtypeStruct...  75.8 us
    unnamed x7, local copies, waits for them, and re-layouts  3.75 us

profile of v1, /device:TPU:0, one launch (start us, length us, event | category | flops | bytes accessed | tf_op | source)
XLA Modules:
  0.0 80.2 jit_solution(13785389302796467318)
XLA Ops:
  0.6 75.8 %ffn_backward.1 = (bf16[256,512]{1,0:T(8,128)(2,1)}, f32[128,1024]{1,0:T(8,128)}, f32[1024,128]{1,0:T(8,128)}) custom-call(bf16[256,512]{1,0:T(8,128)(2,1)} %args_0_.4, bf16[256,512]{1,0:T(8,128)(2,1)} %args_1_.4, bf16[256,1024]{1,0:T(8,128)(2,1)} %args_2_.4, f32[128,1024]{1,0:T(8,128)} %args_3_.4, f32[1,1024]{1,0:T(1,128)} %bitcast.3, f32[1024,128]{1,0:T(8,128)} %args_5_.4, ...), custom_call_target="tpu_custom_call" | custom-call | tf_op jit(solution)/shard_map/ffn_backward/pallas_call | solution.py:297
  76.4 0.0 copy-start.1
  76.5 1.7 %copy.13 = bf16[256,512]{1,0:T(8,128)(2,1)} copy(bf16[256,512]{1,0:T(8,128)(2,1)} %get-tuple-element.6) | data formatting | bytes 524288
  78.2 0.0 copy-done.1
  78.2 0.0 copy-start
  78.2 0.8 copy.14
  79.0 0.4 copy-done
  79.4 0.8 copy.15
Async XLA Ops:
  76.4 1.7 %copy-start.1 = (f32[128,1024]{1,0:T(8,128)S(1)}, f32[128,1024]{1,0:T(8,128)}, u32[]{:S(2)}) copy-start(f32[128,1024]{1,0:T(8,128)} %get-tuple-element.7) | copy-start | bytes 1572868
  78.2 1.2 %copy-start = (f32[1024,128]{1,0:T(8,128)S(1)}, f32[1024,128]{1,0:T(8,128)}, u32[]{:S(2)}) copy-start(f32[1024,128]{1,0:T(8,128)} %get-tuple-element.8) | copy-start | bytes 1572868

commit v2 on v0

v2 whole, which is shorter than its diff:
```python
import math

import jax
import jax.numpy as jnp
from jax import lax
from jax.experimental import pallas as pl
from jax.experimental.pallas import tpu as pltpu
from jax.sharding import PartitionSpec as P

BF = jnp.bfloat16
F32 = jnp.float32
MESH = pl.DeviceIdType.MESH
COPIES = 128


def nt(a, b):
    return lax.dot_general(a, b, (((1,), (1,)), ((), ())), preferred_element_type=F32)


def nn(a, b):
    return lax.dot_general(a, b, (((1,), (0,)), ((), ())), preferred_element_type=F32)


def kernel(
    norm, cot, acts, pre, up, ups, down, dsc,
    gi_out, gu_out, gd_out,
    loc_s, loc_a, xs, xa, pre_r, act_t, wd, wu, da, dr, dpre,
    pd, td1, td2, fd, rd, farxd, nearxd, farxd2, nearxd2, faryd, nearyd, faryd2, nearyd2,
    pu, tu1, tu2, fu, ru, farxu, nearxu, farxu2, nearxu2, faryu, nearyu, faryu2, nearyu2,
    gi, farz, nearz, fz, rz,
    ssem, rsem,
):
    r, f, z = (lax.axis_index(n) for n in ("rep", "fs", "tp"))
    y = lax.div(f, 4)
    xl = lax.rem(lax.div(f, 2), 2)
    c = lax.rem(f, 2)
    x = r * 2 + xl
    oc, ox = 1 - c, 1 - xl

    def dev(dx=0, dy=0, dz=0, core=None):
        nx, ny, nz = (lax.rem(a + d + 4, 4) for a, d in ((x, dx), (y, dy), (z, dz)))
        core = c if core is None else core
        return {
            "rep": lax.div(nx, 2),
            "fs": ny * 4 + lax.rem(nx, 2) * 2 + core,
            "tp": nz,
        }

    def at(a, d):
        return lax.rem(a + d + 4, 4)

    barrier = pltpu.get_barrier_semaphore()
    peers = [dev(dz=d, core=k) for d in (1, -1) for k in (c, oc)]
    peers += [dev(dy=1), dev(dy=-1), dev(dx=1), dev(dx=-1), dev(dx=2), dev(core=oc)]
    for p in peers:
        pl.semaphore_signal(barrier, inc=1, device_id=p, device_id_type=MESH)

    started = []

    def send(src, dst, to):
        k = len(started)
        copy = pltpu.make_async_remote_copy(
            src_ref=src, dst_ref=dst, send_sem=ssem.at[k], recv_sem=rsem.at[k],
            device_id=to, device_id_type=MESH,
        )
        copy.start()
        started.append(copy)
        return copy

    scale = dsc[:, pl.ds(pl.multiple_of(z * 512, 512), 512)]
    scaled = (cot[...].astype(F32) * scale).astype(BF)
    for k in range(2):
        for j in range(2):
            lanes = slice(j * 256 + k * 128, j * 256 + k * 128 + 128)
            loc_s[k, :, j * 128:(j + 1) * 128] = scaled[:, lanes]
            loc_a[k, :, j * 128:(j + 1) * 128] = acts[:, lanes]
    wd[y, xl] = down[...].astype(BF)
    wu[y, xl] = up[...].astype(BF)
    xs[z, 0:256, :] = loc_s[c]
    xa[z, 0:256, :] = loc_a[c]
    pl.semaphore_wait(barrier, len(peers))

    own, other = pl.ds(0, 256), pl.ds(256, 256)

    def z_send(loc, full):
        out = []
        for d in (1, -1):
            out.append(send(loc.at[c], full.at[z, own, :], dev(dz=d)))
            out.append(send(loc.at[oc], full.at[z, other, :], dev(dz=d, core=oc)))
        out.append(send(loc.at[oc], full.at[z, other, :], dev(core=oc)))
        return out

    def z_forward(full, first):
        first[0].wait_recv()
        a = send(full.at[at(z, -1), own, :], full.at[at(z, -1), own, :], dev(dz=1))
        first[3].wait_recv()
        b = send(full.at[at(z, 1), other, :], full.at[at(z, 1), other, :], dev(dz=-1))
        return [first[1], first[2], first[4], a, b]

    def wait_recv(copies):
        for k in copies:
            k.wait_recv()

    def add(a, b):
        return a.astype(F32) + b.astype(F32)

    def relu_sq(v):
        p = jnp.maximum(v.astype(F32), 0.0)
        return (p * p).astype(BF)

    def rows_of(ref, k, xx, lo, n):
        return ref.at[k, xx, pl.ds(lo, n), :]

    def same(ref, to):
        return send(ref, ref, to)

    yn, yp, xn, xp, zn, zp = dev(dy=1), dev(dy=-1), dev(dx=1), dev(dx=-1), dev(dz=1), dev(dz=-1)

    def x_send(w, lo, n, k, h):
        return same(rows_of(w, k, xl, lo + h * n, n), xp if h else xn)

    class Ring:
        def __init__(self, view, me, far, near, nxt, prv):
            self.view, self.me, self.far, self.near = view, me, far, near
            self.nxt, self.prv = nxt, prv

        def start_far(self):
            k = at(self.me, 2)
            self.f = [
                send(self.view(k, 0), self.far.at[0], self.nxt),
                send(self.view(k, 1), self.far.at[1], self.prv),
            ]

        def start_near(self):
            self.n = [
                send(self.view(at(self.me, 1), 1), self.near.at[0, 1], self.nxt),
                send(self.view(at(self.me, -1), 0), self.near.at[1, 0], self.prv),
            ]

        def mid(self):
            for h, d, to in ((0, 1, self.nxt), (1, -1, self.prv)):
                self.f[h].wait_recv()
                v = self.view(at(self.me, d), h)
                v[...] = add(v[...], self.far[h]).astype(BF)
                self.n.append(send(v, self.near.at[h, h], to))

        def result(self):
            wait_recv(self.n)
            for h in range(2):
                v = self.view(self.me, h)
                yield h, add(v[...], self.near[0, h]) + self.near[1, h].astype(F32)

    class Grad:
        def __init__(self, p, t1, t2, fin, rr, farx, nearx, farx2, nearx2, fary, neary, fary2, neary2):
            n = fin.shape[1] // 2
            self.p, self.t1, self.t2, self.fin, self.rr = p, t1, t2, fin, rr
            self.x1 = Ring(
                lambda k, h: p.at[pl.ds(2 * h, 2), lax.rem(k, 2), 0, lax.div(k, 2)],
                x, farx, nearx, xn, xp,
            )
            self.y1 = Ring(lambda k, h: p.at[k, h, 1], y, fary, neary, yn, yp)
            self.y2 = Ring(
                lambda k, h: t1.at[k, pl.ds(h * n, n), :], y, fary2, neary2, yn, yp
            )
            self.x2 = Ring(
                lambda k, h: t2.at[lax.rem(k, 2), lax.div(k, 2), pl.ds(h * n, n), :],
                x, farx2, nearx2, xn, xp,
            )
            self.n = n

        def start(self):
            self.y1.start_far()
            self.x1.start_far()
            self.y1.start_near()
            self.x1.start_near()

        def mid(self):
            self.y1.mid()
            self.x1.mid()

        def second_y(self):
            for h, v in self.x1.result():
                self.t1[2 * h:2 * h + 2] = v.astype(BF)
            self.y2.start_far()
            self.y2.start_near()

        def second_x(self):
            for h, v in self.y1.result():
                self.t2[h] = v.astype(BF)
            self.x2.start_far()
            self.x2.start_near()

        def second_mid(self):
            self.x2.mid()
            self.y2.mid()

        def share(self):
            self.g = []
            for j, ring in ((1, self.x2), (0, self.y2)):
                for h, v in ring.result():
                    self.fin[j, h * self.n:(h + 1) * self.n, :] = v.astype(BF)
                self.g.append(send(self.fin.at[j], self.rr.at[j], dev(dx=2)))

        def store(self, out):
            for j in range(2):
                out[j, r] = self.fin[j].astype(F32) * norm
            wait_recv(self.g)
            for j in range(2):
                out[j, 1 - r] = self.rr[j].astype(F32) * norm

    gd = Grad(pd, td1, td2, fd, rd, farxd, nearxd, farxd2, nearxd2, faryd, nearyd, faryd2, nearyd2)
    gu = Grad(pu, tu1, tu2, fu, ru, farxu, nearxu, farxu2, nearxu2, faryu, nearyu, faryu2, nearyu2)
    scope = jax.named_scope

    with scope("a_first_sends"):
        s1 = z_send(loc_s, xs)
        wd1 = [
            same(rows_of(wd, y, xl, 512 * h, 512), to)
            for h, to in ((0, yn), (1, yp), (1, yn), (0, yp))
        ]
        wdx = {d: [] for d in (0, 1, -1, 2)}
        wdx[0] = [x_send(wd, 0, 512, y, h) for h in range(2)]
        pre1 = send(pre, pre_r, dev(core=oc))
        wu_x = [x_send(wu, 64, 32, y, h) for h in range(2)]
    with scope("b_wd_first"):
        wd1[0].wait_recv()
        wd2 = [same(rows_of(wd, at(y, -1), xl, 0, 512), yn)]
        wdx[-1].append(x_send(wd, 0, 512, at(y, -1), 0))
        wd1[1].wait_recv()
        wd2.append(same(rows_of(wd, at(y, 1), xl, 512, 512), yp))
        wdx[1].append(x_send(wd, 0, 512, at(y, 1), 1))
    with scope("c_z_forward"):
        s2 = z_forward(xs, s1)
        a1 = z_send(loc_a, xa)
    with scope("d_wd_second"):
        wd1[2].wait_recv()
        wdx[-1].append(x_send(wd, 0, 512, at(y, -1), 1))
        wd1[3].wait_recv()
        wdx[1].append(x_send(wd, 0, 512, at(y, 1), 0))
        wuy = [same(rows_of(wu, y, xl, 0, 64), to) for to in (yn, yp)]
        wuo = [same(rows_of(wu, y, xl, 64, 64), to) for to in (yn, yp)]
    with scope("e_act"):
        act_t[:, 0:256] = relu_sq(pre[...]).T
        pre1.wait_recv()
        act_t[:, 256:512] = relu_sq(pre_r[...]).T
    with scope("f_wd_third"):
        for h in range(2):
            wd2[h].wait_recv()
            wdx[2].append(x_send(wd, 0, 512, at(y, 2), h))
    with scope("g_scaled_wait"):
        wait_recv(s2)
    with scope("h_grad_down"):
        for k in range(4):
            part = nn(act_t[...], xs[k])
            for j in range(2):
                pd[k, j] = part[:, j * 128:(j + 1) * 128].astype(BF).reshape(2, 2, 256, 128)
        gd.start()
    with scope("i_wu_second"):
        wux = [x_send(wu, 0, 32, y, h) for h in range(2)]
        wuo2 = []
        for h in range(2):
            wu_x[h].wait_recv()
            piece = rows_of(wu, y, ox, 64 + 32 * h, 32)
            wuo2 += [same(piece, yn), same(piece, yp)]
        wuf = []
        for h, to, d in ((0, yn, -1), (1, yp, 1)):
            wuy[h].wait_recv()
            k = at(y, d)
            wuf.append(same(rows_of(wu, k, xl, 32 * h, 32), to))
            wux += [x_send(wu, 0, 32, k, 0), x_send(wu, 0, 32, k, 1)]
    with scope("j_acts_forward"):
        a2 = z_forward(xa, a1)
    dax = []
    for d in (0, 1, -1, 2):
        with scope("k_wd_wait"):
            wait_recv(wdx[d])
        with scope("l_d_act"):
            k = at(y, d)
            w = jnp.concatenate([wd[k, 0], wd[k, 1]], axis=1)
            for h in (0, 1):
                term = nt(xs[k, h * 256:(h + 1) * 256, :], w)
                da[h] = term if d == 0 else da[h] + term
                if d == 2:
                    dax.append(send(da.at[h], dr.at[1 - h], dev(core=oc)))
    with scope("m_wu_third"):
        wuo[0].wait_recv()
        wug = [same(rows_of(wu, at(y, -1), xl, 64, 64), yn)]
        for h in range(2):
            wuo2[2 * h + 1].wait_recv()
            wug.append(same(rows_of(wu, at(y, 1), ox, 64 + 32 * h, 32), yp))
        for h in range(2):
            wuf[h].wait_recv()
            wux.append(x_send(wu, 0, 32, at(y, 2), h))
    with scope("n_dpre"):
        for h in (1, 0):
            dax[1 - h].wait_recv()
            src = pre if h == 0 else pre_r
            pos = jnp.maximum(src[...].astype(F32), 0.0)
            dpre[h * 256:(h + 1) * 256, :] = (2.0 * pos * (da[h] + dr[h]) * ups[...]).astype(BF)
    with scope("o_acts_wait"):
        wait_recv(a2)
    with scope("p_grad_up"):
        for k in range(4):
            part = nn(xa[k].T, dpre[...])
            for j in range(2):
                pu[k, j] = part[j * 128:(j + 1) * 128, :].astype(BF).reshape(2, 2, 32, 1024)
        gu.start()
    with scope("q_gd_mid"):
        gd.mid()
    with scope("r_wu_wait"):
        wait_recv(wux)
        wait_recv(wuo[1:] + [wuo2[0], wuo2[2]] + wug)
    zr = Ring(lambda k, h: gi.at[k, pl.ds(256 * h, 256), :], z, farz, nearz, zn, zp)
    with scope("s_grad_in"):
        for d in (2, 1, -1, 0):
            k = at(z, d)
            gi[k] = nt(dpre[...], wu[k].reshape(256, 1024)).astype(BF)
            if d == 2:
                zr.start_far()
            if d == -1:
                zr.start_near()
    with scope("t_gd_second"):
        gd.second_x()
        gd.second_y()
    with scope("u_gu_mid"):
        gu.mid()
    with scope("v_z_mid"):
        zr.mid()
    with scope("w_gd_second_mid"):
        gd.second_mid()
    with scope("x_gu_second"):
        gu.second_x()
        gu.second_y()
    with scope("y_gd_share"):
        gd.share()
    with scope("z_gi"):
        for h, v in zr.result():
            fz[h] = v.astype(BF)
        gx = send(fz.at[1], rz, dev(core=oc))
    with scope("za_gu_second_mid"):
        gu.second_mid()
    with scope("zb_gi_out"):
        gx.wait_recv()
        for j in range(2):
            lanes = pl.ds(pl.multiple_of(j * 256 + c * 128, 128), 128)
            gi_out[:, lanes] = fz[0, :, j * 128:(j + 1) * 128]
            lanes = pl.ds(pl.multiple_of(j * 256 + oc * 128, 128), 128)
            gi_out[:, lanes] = rz[:, j * 128:(j + 1) * 128]
    with scope("zc_gd_out"):
        gd.store(gd_out)
    with scope("zd_gu_share"):
        gu.share()
    with scope("ze_gu_out"):
        gu.store(gu_out)
    with scope("zf_drain"):
        for copy in started:
            copy.wait_send()


def body(acts, cotangent, pre_act, up_store, up_scale, down_store, down_scale):
    tokens = acts.shape[0] * lax.axis_size("fs") * lax.axis_size("rep")
    norm = 1.0 / math.sqrt(tokens)

    def vm(*shape, dtype=BF):
        return pltpu.VMEM(shape, dtype)

    def grad_bufs(n, m):
        out = [vm(4, 2, 2, 2, n, m), vm(4, n, m), vm(2, 2, n, m), vm(2, n, m), vm(2, n, m)]
        for lead, rows in (((2,), n), ((), n // 2)) * 2:
            out += [vm(2, *lead, rows, m), vm(2, 2, *lead, rows, m)]
        return out

    spec = pl.BlockSpec(memory_space=pltpu.VMEM)

    def call(*args):
        return kernel(norm, *args)

    gi, gu, gd = pl.pallas_call(
        call,
        name="ffn_backward",
        out_shape=(
            jax.ShapeDtypeStruct((256, 512), BF),
            jax.ShapeDtypeStruct((2, 2, 32, 1024), F32),
            jax.ShapeDtypeStruct((2, 2, 256, 128), F32),
        ),
        in_specs=[spec] * 7,
        out_specs=(spec,) * 3,
        scratch_shapes=[
            vm(2, 256, 256), vm(2, 256, 256), vm(4, 512, 256), vm(4, 512, 256),
            vm(256, 1024), vm(1024, 512), vm(4, 2, 1024, 128), vm(4, 2, 128, 1024),
            vm(2, 256, 1024, dtype=F32), vm(2, 256, 1024, dtype=F32), vm(512, 1024),
            *grad_bufs(256, 128),
            *grad_bufs(32, 1024),
            vm(4, 512, 256), vm(2, 256, 256), vm(2, 2, 256, 256), vm(2, 256, 256), vm(256, 256),
            pltpu.SemaphoreType.DMA((COPIES,)),
            pltpu.SemaphoreType.DMA((COPIES,)),
        ],
        compiler_params=pltpu.CompilerParams(
            collective_id=0, has_side_effects=True, vmem_limit_bytes=56 * 1024 * 1024
        ),
    )(
        cotangent, acts, pre_act, up_store, up_scale.reshape(1, -1),
        down_store, down_scale.reshape(1, -1),
    )
    return gi, gu.reshape(up_store.shape), gd.reshape(down_store.shape)


def solution(mesh):
    return jax.shard_map(
        body,
        mesh=mesh,
        in_specs=(
            P(("rep", "fs"), "tp"),
            P(("rep", "fs"), "tp"),
            P(("rep", "fs"), "tp"),
            P("fs", "tp"),
            P("tp"),
            P("tp", "fs"),
            P(),
        ),
        out_specs=(P(("rep", "fs"), "tp"), P("fs", "tp"), P("tp", "fs")),
        check_vma=False,
    )
```

time: 301 us -> 75.7 us (0.25)
  the two profiles are of different devices: /device:TPU:0 before, /device:TPU:2 now
where the time goes in v2:
time: 75.7 us; the launch traced here: 75.5 us
  Pallas kernels  71.1 us (94%)
  local copies, waits for them, and re-layouts  3.75 us (5%)
    pallas_call x1, Pallas kernels, body(): pl.pallas_call(call, name='ffn_backward', out_shape=(jax.ShapeDtypeStruct...  71.1 us
    unnamed x7, local copies, waits for them, and re-layouts  3.75 us

profile of v2, /device:TPU:2, one launch (start us, length us, event | category | flops | bytes accessed | tf_op | source)
XLA Modules:
  0.0 75.5 jit_solution(4191973221443645742)
XLA Ops:
  0.6 71.1 %ffn_backward.1 = (bf16[256,512]{1,0:T(8,128)(2,1)}, f32[2,2,32,1024]{3,2,1,0:T(8,128)}, f32[2,2,256,128]{3,2,1,0:T(8,128)}) custom-call(bf16[256,512]{1,0:T(8,128)(2,1)} %args_0_.4, bf16[256,512]{1,0:T(8,128)(2,1)} %args_1_.4, bf16[256,1024]{1,0:T(8,128)(2,1)} %args_2_.4, f32[128,1024]{1,0:T(8,128)} %args_3_.4, f32[1,1024]{1,0:T(1,128)} %bitcast.7, ...), custom_call_target="tpu_custom_call" | custom-call | tf_op jit(solution)/shard_map/ffn_backward/pallas_call | solution.py:378
  71.7 0.0 copy-start.1
  71.7 1.7 %copy.13 = bf16[256,512]{1,0:T(8,128)(2,1)} copy(bf16[256,512]{1,0:T(8,128)(2,1)} %get-tuple-element.12) | data formatting | bytes 524288
  73.5 0.0 copy-done.1
  73.5 0.0 copy-start
  73.5 0.8 %copy.14 = f32[128,1024]{1,0:T(8,128)} copy(f32[128,1024]{1,0:T(8,128)S(1)} %bitcast.5) | data formatting | bytes 1048576
  74.3 0.4 copy-done
  74.7 0.8 %copy.15 = f32[1024,128]{1,0:T(8,128)} copy(f32[1024,128]{1,0:T(8,128)S(1)} %bitcast.4) | data formatting | bytes 1048576
Async XLA Ops:
  71.7 1.7 %copy-start.1 = (f32[2,2,32,1024]{3,2,1,0:T(8,128)S(1)}, f32[2,2,32,1024]{3,2,1,0:T(8,128)}, u32[]{:S(2)}) copy-start(f32[2,2,32,1024]{3,2,1,0:T(8,128)} %get-tuple-element.7) | copy-start | bytes 1572868
  73.5 1.2 %copy-start = (f32[2,2,256,128]{3,2,1,0:T(8,128)S(1)}, f32[2,2,256,128]{3,2,1,0:T(8,128)}, u32[]{:S(2)}) copy-start(f32[2,2,256,128]{3,2,1,0:T(8,128)} %get-tuple-element.8) | copy-start | bytes 1572868

commit v3 on v2

--- a/solution.py
+++ b/solution.py
@@ -22,13 +22,14 @@
 
 
 def kernel(
-    norm, cot, acts, pre, up, ups, down, dsc,
+    norm, cot_h, acts_h, pre_h, up_h, ups_h, down_h, dsc_h,
     gi_out, gu_out, gd_out,
     loc_s, loc_a, xs, xa, pre_r, act_t, wd, wu, da, dr, dpre,
-    pd, td1, td2, fd, rd, farxd, nearxd, farxd2, nearxd2, faryd, nearyd, faryd2, nearyd2,
-    pu, tu1, tu2, fu, ru, farxu, nearxu, farxu2, nearxu2, faryu, nearyu, faryu2, nearyu2,
+    pd, td1, td2, fd, rd, farxd, nearxd, gotd, rawd, vd, faryd, nearyd, faryd2, nearyd2,
+    pu, tu1, tu2, fu, ru, farxu, nearxu, gotu, rawu, vu, faryu, nearyu, faryu2, nearyu2,
     gi, farz, nearz, fz, rz,
-    ssem, rsem,
+    cot, acts, pre, up, ups, down, dsc,
+    ssem, rsem, lsem,
 ):
     r, f, z = (lax.axis_index(n) for n in ("rep", "fs", "tp"))
     y = lax.div(f, 4)
@@ -55,6 +56,13 @@
     for p in peers:
         pl.semaphore_signal(barrier, inc=1, device_id=p, device_id_type=MESH)
 
+    loads = {}
+    for i, (n, src, dst) in enumerate((
+        ("dsc", dsc_h, dsc), ("cot", cot_h, cot), ("down", down_h, down), ("acts", acts_h, acts),
+        ("up", up_h, up), ("pre", pre_h, pre), ("ups", ups_h, ups),
+    )):
+        loads[n] = pltpu.make_async_copy(src, dst, lsem.at[i])
+        loads[n].start()
     started = []
 
     def send(src, dst, to):
@@ -67,35 +75,46 @@
         started.append(copy)
         return copy
 
+    def split(dst, v):
+        for k in range(2):
+            for j in range(2):
+                lanes = slice(j * 256 + k * 128, j * 256 + k * 128 + 128)
+                dst[k, :, j * 128:(j + 1) * 128] = v[:, lanes]
+
+    loads["dsc"].wait()
     scale = dsc[:, pl.ds(pl.multiple_of(z * 512, 512), 512)]
-    scaled = (cot[...].astype(F32) * scale).astype(BF)
-    for k in range(2):
-        for j in range(2):
-            lanes = slice(j * 256 + k * 128, j * 256 + k * 128 + 128)
-            loc_s[k, :, j * 128:(j + 1) * 128] = scaled[:, lanes]
-            loc_a[k, :, j * 128:(j + 1) * 128] = acts[:, lanes]
+    loads["cot"].wait()
+    split(loc_s, (cot[...].astype(F32) * scale).astype(BF))
+    xs[z, 0:256, :] = loc_s[c]
+    loads["down"].wait()
     wd[y, xl] = down[...].astype(BF)
+    loads["acts"].wait()
+    split(loc_a, acts[...])
+    xa[z, 0:256, :] = loc_a[c]
+    loads["up"].wait()
     wu[y, xl] = up[...].astype(BF)
-    xs[z, 0:256, :] = loc_s[c]
-    xa[z, 0:256, :] = loc_a[c]
+    loads["pre"].wait()
+    loads["ups"].wait()
     pl.semaphore_wait(barrier, len(peers))
 
     own, other = pl.ds(0, 256), pl.ds(256, 256)
 
     def z_send(loc, full):
-        out = []
-        for d in (1, -1):
-            out.append(send(loc.at[c], full.at[z, own, :], dev(dz=d)))
-            out.append(send(loc.at[oc], full.at[z, other, :], dev(dz=d, core=oc)))
-        out.append(send(loc.at[oc], full.at[z, other, :], dev(core=oc)))
-        return out
+        def go(k, dz):
+            part = own if k is c else other
+            return send(loc.at[k], full.at[z, part, :], dev(dz=dz, core=k))
+
+        return [go(c, 1), go(oc, -1), go(oc, 1), go(c, -1), go(oc, 0)]
 
     def z_forward(full, first):
         first[0].wait_recv()
-        a = send(full.at[at(z, -1), own, :], full.at[at(z, -1), own, :], dev(dz=1))
-        first[3].wait_recv()
-        b = send(full.at[at(z, 1), other, :], full.at[at(z, 1), other, :], dev(dz=-1))
-        return [first[1], first[2], first[4], a, b]
+        a = same(full.at[at(z, -1), own, :], dev(dz=1))
+        first[1].wait_recv()
+        b = same(full.at[at(z, 1), other, :], dev(dz=-1))
+        return first[2:] + [a, b]
+
+    def same(ref, to):
+        return send(ref, ref, to)
 
     def wait_recv(copies):
         for k in copies:
@@ -110,9 +129,6 @@
 
     def rows_of(ref, k, xx, lo, n):
         return ref.at[k, xx, pl.ds(lo, n), :]
-
-    def same(ref, to):
-        return send(ref, ref, to)
 
     yn, yp, xn, xp, zn, zp = dev(dy=1), dev(dy=-1), dev(dx=1), dev(dx=-1), dev(dz=1), dev(dz=-1)
 
@@ -151,9 +167,10 @@
                 yield h, add(v[...], self.near[0, h]) + self.near[1, h].astype(F32)
 
     class Grad:
-        def __init__(self, p, t1, t2, fin, rr, farx, nearx, farx2, nearx2, fary, neary, fary2, neary2):
-            n = fin.shape[1] // 2
+        def __init__(self, p, t1, t2, fin, rr, farx, nearx, got, raw, vb, fary, neary, fary2, neary2):
+            n = fin.shape[0] // 2
             self.p, self.t1, self.t2, self.fin, self.rr = p, t1, t2, fin, rr
+            self.got, self.raw, self.vb = got, raw, vb
             self.x1 = Ring(
                 lambda k, h: p.at[pl.ds(2 * h, 2), lax.rem(k, 2), 0, lax.div(k, 2)],
                 x, farx, nearx, xn, xp,
@@ -162,10 +179,6 @@
             self.y2 = Ring(
                 lambda k, h: t1.at[k, pl.ds(h * n, n), :], y, fary2, neary2, yn, yp
             )
-            self.x2 = Ring(
-                lambda k, h: t2.at[lax.rem(k, 2), lax.div(k, 2), pl.ds(h * n, n), :],
-                x, farx2, nearx2, xn, xp,
-            )
             self.n = n
 
         def start(self):
@@ -185,31 +198,42 @@
             self.y2.start_near()
 
         def second_x(self):
+            t2, got, raw = self.t2, self.got, self.raw
             for h, v in self.y1.result():
-                self.t2[h] = v.astype(BF)
-            self.x2.start_far()
-            self.x2.start_near()
-
-        def second_mid(self):
-            self.x2.mid()
-            self.y2.mid()
+                t2[h] = v.astype(BF)
+            self.c1 = [
+                send(t2.at[xl, r], got.at[0], xn),
+                send(t2.at[xl, 1 - r], got.at[1], xp),
+            ]
+            self.c2 = [
+                send(t2.at[ox, 1 - mine], raw.at[0], xn),
+                send(t2.at[ox, 1 - mine], raw.at[1], xp),
+            ]
+
+        def second_x_mid(self):
+            wait_recv(self.c1)
+            v = self.t2.at[ox, mine]
+            v[...] = (add(self.got[0], self.got[1]) + v[...].astype(F32)).astype(BF)
+            self.c2 += [send(v, self.vb.at[0], xn), send(v, self.vb.at[1], xp)]
+
+        def store_second(self, out):
+            wait_recv(self.c2)
+            out[1, 1 - r] = add(self.vb[0], self.raw[1]) * norm
+            out[1, r] = add(self.vb[1], self.raw[0]) * norm
 
         def share(self):
-            self.g = []
-            for j, ring in ((1, self.x2), (0, self.y2)):
-                for h, v in ring.result():
-                    self.fin[j, h * self.n:(h + 1) * self.n, :] = v.astype(BF)
-                self.g.append(send(self.fin.at[j], self.rr.at[j], dev(dx=2)))
-
-        def store(self, out):
-            for j in range(2):
-                out[j, r] = self.fin[j].astype(F32) * norm
-            wait_recv(self.g)
-            for j in range(2):
-                out[j, 1 - r] = self.rr[j].astype(F32) * norm
-
-    gd = Grad(pd, td1, td2, fd, rd, farxd, nearxd, farxd2, nearxd2, faryd, nearyd, faryd2, nearyd2)
-    gu = Grad(pu, tu1, tu2, fu, ru, farxu, nearxu, farxu2, nearxu2, faryu, nearyu, faryu2, nearyu2)
+            for h, v in self.y2.result():
+                self.fin[h * self.n:(h + 1) * self.n, :] = v.astype(BF)
+            self.g = send(self.fin, self.rr, dev(dx=2))
+
+        def store_first(self, out):
+            out[0, r] = self.fin[...].astype(F32) * norm
+            self.g.wait_recv()
+            out[0, 1 - r] = self.rr[...].astype(F32) * norm
+
+    mine = r * xl + (1 - r) * ox
+    gd = Grad(pd, td1, td2, fd, rd, farxd, nearxd, gotd, rawd, vd, faryd, nearyd, faryd2, nearyd2)
+    gu = Grad(pu, tu1, tu2, fu, ru, farxu, nearxu, gotu, rawu, vu, faryu, nearyu, faryu2, nearyu2)
     scope = jax.named_scope
 
     with scope("a_first_sends"):
@@ -239,6 +263,11 @@
         wdx[1].append(x_send(wd, 0, 512, at(y, 1), 0))
         wuy = [same(rows_of(wu, y, xl, 0, 64), to) for to in (yn, yp)]
         wuo = [same(rows_of(wu, y, xl, 64, 64), to) for to in (yn, yp)]
+        wuo2 = []
+        for h in range(2):
+            wu_x[h].wait_recv()
+            piece = rows_of(wu, y, ox, 64 + 32 * h, 32)
+            wuo2 += [same(piece, yn), same(piece, yp)]
     with scope("e_act"):
         act_t[:, 0:256] = relu_sq(pre[...]).T
         pre1.wait_recv()
@@ -247,6 +276,7 @@
         for h in range(2):
             wd2[h].wait_recv()
             wdx[2].append(x_send(wd, 0, 512, at(y, 2), h))
+        wux = [x_send(wu, 0, 32, y, h) for h in range(2)]
     with scope("g_scaled_wait"):
         wait_recv(s2)
     with scope("h_grad_down"):
@@ -254,14 +284,10 @@
             part = nn(act_t[...], xs[k])
             for j in range(2):
                 pd[k, j] = part[:, j * 128:(j + 1) * 128].astype(BF).reshape(2, 2, 256, 128)
-        gd.start()
+        gd.y1.start_far()
+        gd.x1.start_far()
+        gd.x1.start_near()
     with scope("i_wu_second"):
-        wux = [x_send(wu, 0, 32, y, h) for h in range(2)]
-        wuo2 = []
-        for h in range(2):
-            wu_x[h].wait_recv()
-            piece = rows_of(wu, y, ox, 64 + 32 * h, 32)
-            wuo2 += [same(piece, yn), same(piece, yp)]
         wuf = []
         for h, to, d in ((0, yn, -1), (1, yp, 1)):
             wuy[h].wait_recv()
@@ -288,9 +314,7 @@
         for h in range(2):
             wuo2[2 * h + 1].wait_recv()
             wug.append(same(rows_of(wu, at(y, 1), ox, 64 + 32 * h, 32), yp))
-        for h in range(2):
-            wuf[h].wait_recv()
-            wux.append(x_send(wu, 0, 32, at(y, 2), h))
+        gd.y1.start_near()
     with scope("n_dpre"):
         for h in (1, 0):
             dax[1 - h].wait_recv()
@@ -304,13 +328,17 @@
             part = nn(xa[k].T, dpre[...])
             for j in range(2):
                 pu[k, j] = part[j * 128:(j + 1) * 128, :].astype(BF).reshape(2, 2, 32, 1024)
+    with scope("q_gd_mid"):
+        for h in range(2):
+            wuf[h].wait_recv()
+            wux.append(x_send(wu, 0, 32, at(y, 2), h))
+        gd.x1.mid()
+        gd.y1.mid()
         gu.start()
-    with scope("q_gd_mid"):
-        gd.mid()
+    zr = Ring(lambda k, h: gi.at[k, pl.ds(256 * h, 256), :], z, farz, nearz, zn, zp)
     with scope("r_wu_wait"):
         wait_recv(wux)
         wait_recv(wuo[1:] + [wuo2[0], wuo2[2]] + wug)
-    zr = Ring(lambda k, h: gi.at[k, pl.ds(256 * h, 256), :], z, farz, nearz, zn, zp)
     with scope("s_grad_in"):
         for d in (2, 1, -1, 0):
             k = at(z, d)
@@ -320,39 +348,45 @@
             if d == -1:
                 zr.start_near()
     with scope("t_gd_second"):
+        gd.second_y()
         gd.second_x()
-        gd.second_y()
     with scope("u_gu_mid"):
         gu.mid()
     with scope("v_z_mid"):
         zr.mid()
     with scope("w_gd_second_mid"):
-        gd.second_mid()
-    with scope("x_gu_second"):
-        gu.second_x()
-        gu.second_y()
+        gd.y2.mid()
+        gd.second_x_mid()
     with scope("y_gd_share"):
         gd.share()
+    with scope("x_gu_second"):
+        gu.second_y()
+        gu.second_x()
     with scope("z_gi"):
         for h, v in zr.result():
             fz[h] = v.astype(BF)
         gx = send(fz.at[1], rz, dev(core=oc))
-    with scope("za_gu_second_mid"):
-        gu.second_mid()
-    with scope("zb_gi_out"):
+    with scope("za_gu_y2_mid"):
+        gu.y2.mid()
+    with scope("zb_gu_x2_mid"):
+        gu.second_x_mid()
+    with scope("zc_gi_out"):
         gx.wait_recv()
         for j in range(2):
             lanes = pl.ds(pl.multiple_of(j * 256 + c * 128, 128), 128)
             gi_out[:, lanes] = fz[0, :, j * 128:(j + 1) * 128]
             lanes = pl.ds(pl.multiple_of(j * 256 + oc * 128, 128), 128)
             gi_out[:, lanes] = rz[:, j * 128:(j + 1) * 128]
-    with scope("zc_gd_out"):
-        gd.store(gd_out)
     with scope("zd_gu_share"):
         gu.share()
-    with scope("ze_gu_out"):
-        gu.store(gu_out)
-    with scope("zf_drain"):
+    with scope("ze_gd_out"):
+        gd.store_first(gd_out)
+        gd.store_second(gd_out)
+    with scope("zf_gu_out"):
+        gu.store_second(gu_out)
+    with scope("zg_gu_out"):
+        gu.store_first(gu_out)
+    with scope("zh_drain"):
         for copy in started:
             copy.wait_send()
 
@@ -365,10 +399,11 @@
         return pltpu.VMEM(shape, dtype)
 
     def grad_bufs(n, m):
-        out = [vm(4, 2, 2, 2, n, m), vm(4, n, m), vm(2, 2, n, m), vm(2, n, m), vm(2, n, m)]
-        for lead, rows in (((2,), n), ((), n // 2)) * 2:
-            out += [vm(2, *lead, rows, m), vm(2, 2, *lead, rows, m)]
-        return out
+        return [
+            vm(4, 2, 2, 2, n, m), vm(4, n, m), vm(2, 2, n, m), vm(n, m), vm(n, m),
+            vm(2, 2, n, m), vm(2, 2, 2, n, m), vm(2, n, m), vm(2, n, m), vm(2, n, m),
+            vm(2, 2, n, m), vm(2, 2, 2, n, m), vm(2, n // 2, m), vm(2, 2, n // 2, m),
+        ]
 
     spec = pl.BlockSpec(memory_space=pltpu.VMEM)
 
@@ -383,7 +418,7 @@
             jax.ShapeDtypeStruct((2, 2, 32, 1024), F32),
             jax.ShapeDtypeStruct((2, 2, 256, 128), F32),
         ),
-        in_specs=[spec] * 7,
+        in_specs=[pl.BlockSpec(memory_space=pl.ANY)] * 7,
         out_specs=(spec,) * 3,
         scratch_shapes=[
             vm(2, 256, 256), vm(2, 256, 256), vm(4, 512, 256), vm(4, 512, 256),
@@ -392,8 +427,11 @@
             *grad_bufs(256, 128),
             *grad_bufs(32, 1024),
             vm(4, 512, 256), vm(2, 256, 256), vm(2, 2, 256, 256), vm(2, 256, 256), vm(256, 256),
+            vm(256, 512), vm(256, 512), vm(256, 1024), vm(128, 1024, dtype=F32),
+            vm(1, 1024, dtype=F32), vm(1024, 128, dtype=F32), vm(1, 2048, dtype=F32),
             pltpu.SemaphoreType.DMA((COPIES,)),
             pltpu.SemaphoreType.DMA((COPIES,)),
+            pltpu.SemaphoreType.DMA((7,)),
         ],
         compiler_params=pltpu.CompilerParams(
             collective_id=0, has_side_effects=True, vmem_limit_bytes=56 * 1024 * 1024

time: 75.7 us -> 68 us (0.90)
  the two profiles are of different devices: /device:TPU:2 before, /device:TPU:0 now
where the time goes in v3:
time: 68 us; the launch traced here: 67.7 us
  Pallas kernels  63.3 us (93%)
  local copies, waits for them, and re-layouts  3.75 us (6%)
    pallas_call x1, Pallas kernels, body(): pl.pallas_call(call, name='ffn_backward', out_shape=(jax.ShapeDtypeStruct...  63.3 us
    unnamed x7, local copies, waits for them, and re-layouts  3.75 us

profile of v3, /device:TPU:0, one launch (start us, length us, event | category | flops | bytes accessed | tf_op | source)
XLA Modules:
  0.0 67.7 jit_solution(1001436986597137920)
XLA Ops:
  0.6 63.3 %ffn_backward.1 = (bf16[256,512]{1,0:T(8,128)(2,1)}, f32[2,2,32,1024]{3,2,1,0:T(8,128)}, f32[2,2,256,128]{3,2,1,0:T(8,128)}) custom-call(bf16[256,512]{1,0:T(8,128)(2,1)} %args_0_.4, bf16[256,512]{1,0:T(8,128)(2,1)} %args_1_.4, bf16[256,1024]{1,0:T(8,128)(2,1)} %args_2_.4, f32[128,1024]{1,0:T(8,128)} %args_3_.4, f32[1,1024]{1,0:T(1,128)} %bitcast.7, ...), custom_call_target="tpu_custom_call" | custom-call | tf_op jit(solution)/shard_map/ffn_backward/pallas_call | solution.py:413
  64.0 0.0 copy-start.1
  64.0 1.7 %copy.13 = bf16[256,512]{1,0:T(8,128)(2,1)} copy(bf16[256,512]{1,0:T(8,128)(2,1)} %get-tuple-element.12) | data formatting | bytes 524288
  65.7 0.0 copy-done.1
  65.7 0.0 copy-start
  65.7 0.8 %copy.14 = f32[128,1024]{1,0:T(8,128)} copy(f32[128,1024]{1,0:T(8,128)S(1)} %bitcast.5) | data formatting | bytes 1048576
  66.5 0.4 copy-done
  67.0 0.8 %copy.15 = f32[1024,128]{1,0:T(8,128)} copy(f32[1024,128]{1,0:T(8,128)S(1)} %bitcast.4) | data formatting | bytes 1048576
Async XLA Ops:
  64.0 1.7 %copy-start.1 = (f32[2,2,32,1024]{3,2,1,0:T(8,128)S(1)}, f32[2,2,32,1024]{3,2,1,0:T(8,128)}, u32[]{:S(2)}) copy-start(f32[2,2,32,1024]{3,2,1,0:T(8,128)} %get-tuple-element.7) | copy-start | bytes 1572868
  65.7 1.2 %copy-start = (f32[2,2,256,128]{3,2,1,0:T(8,128)S(1)}, f32[2,2,256,128]{3,2,1,0:T(8,128)}, u32[]{:S(2)}) copy-start(f32[2,2,256,128]{3,2,1,0:T(8,128)} %get-tuple-element.8) | copy-start | bytes 1572868

commit v4 on v3

--- a/solution.py
+++ b/solution.py
@@ -10,7 +10,8 @@
 BF = jnp.bfloat16
 F32 = jnp.float32
 MESH = pl.DeviceIdType.MESH
-COPIES = 128
+RECVS = 57
+SENT_ROWS = 52736
 
 
 def nt(a, b):
@@ -29,7 +30,7 @@
     pu, tu1, tu2, fu, ru, farxu, nearxu, gotu, rawu, vu, faryu, nearyu, faryu2, nearyu2,
     gi, farz, nearz, fz, rz,
     cot, acts, pre, up, ups, down, dsc,
-    ssem, rsem, lsem,
+    sent, ssem, rsem, lsem,
 ):
     r, f, z = (lax.axis_index(n) for n in ("rep", "fs", "tp"))
     y = lax.div(f, 4)
@@ -65,15 +66,33 @@
         loads[n].start()
     started = []
 
-    def send(src, dst, to):
-        k = len(started)
+    recvs = [0]
+
+    def blank(rows):
+        return sent.at[pl.ds(0, rows), :]
+
+    def rows_in(ref):
+        return math.prod(ref.shape) * jnp.dtype(ref.dtype).itemsize // 256
+
+    class Group:
+        def __init__(self):
+            self.k, self.rows = recvs[0], 0
+            recvs[0] += 1
+
+        def wait_recv(self):
+            d = blank(self.rows)
+            pltpu.make_async_copy(d, d, rsem.at[self.k]).wait()
+
+    def send(src, dst, to, group=None):
+        group = group or Group()
+        group.rows += rows_in(src)
         copy = pltpu.make_async_remote_copy(
-            src_ref=src, dst_ref=dst, send_sem=ssem.at[k], recv_sem=rsem.at[k],
+            src_ref=src, dst_ref=dst, send_sem=ssem, recv_sem=rsem.at[group.k],
             device_id=to, device_id_type=MESH,
         )
         copy.start()
-        started.append(copy)
-        return copy
+        started.append(rows_in(src))
+        return group
 
     def split(dst, v):
         for k in range(2):
@@ -99,26 +118,28 @@
 
     own, other = pl.ds(0, 256), pl.ds(256, 256)
 
+    def same(ref, to, group=None):
+        return send(ref, ref, to, group)
+
     def z_send(loc, full):
-        def go(k, dz):
+        rest = Group()
+
+        def go(k, dz, group=None):
             part = own if k is c else other
-            return send(loc.at[k], full.at[z, part, :], dev(dz=dz, core=k))
-
-        return [go(c, 1), go(oc, -1), go(oc, 1), go(c, -1), go(oc, 0)]
-
-    def z_forward(full, first):
+            return send(loc.at[k], full.at[z, part, :], dev(dz=dz, core=k), group)
+
+        first = [go(c, 1), go(oc, -1)]
+        for k, dz in ((oc, 1), (c, -1), (oc, 0)):
+            go(k, dz, rest)
+        return first, rest
+
+    def z_forward(full, sends):
+        first, rest = sends
         first[0].wait_recv()
-        a = same(full.at[at(z, -1), own, :], dev(dz=1))
+        same(full.at[at(z, -1), own, :], dev(dz=1), rest)
         first[1].wait_recv()
-        b = same(full.at[at(z, 1), other, :], dev(dz=-1))
-        return first[2:] + [a, b]
-
-    def same(ref, to):
-        return send(ref, ref, to)
-
-    def wait_recv(copies):
-        for k in copies:
-            k.wait_recv()
+        same(full.at[at(z, 1), other, :], dev(dz=-1), rest)
+        return rest
 
     def add(a, b):
         return a.astype(F32) + b.astype(F32)
@@ -132,8 +153,8 @@
 
     yn, yp, xn, xp, zn, zp = dev(dy=1), dev(dy=-1), dev(dx=1), dev(dx=-1), dev(dz=1), dev(dz=-1)
 
-    def x_send(w, lo, n, k, h):
-        return same(rows_of(w, k, xl, lo + h * n, n), xp if h else xn)
+    def x_send(w, lo, n, k, h, group=None):
+        return same(rows_of(w, k, xl, lo + h * n, n), xp if h else xn, group)
 
     class Ring:
         def __init__(self, view, me, far, near, nxt, prv):
@@ -148,20 +169,19 @@
             ]
 
         def start_near(self):
-            self.n = [
-                send(self.view(at(self.me, 1), 1), self.near.at[0, 1], self.nxt),
-                send(self.view(at(self.me, -1), 0), self.near.at[1, 0], self.prv),
-            ]
+            self.n = Group()
+            send(self.view(at(self.me, 1), 1), self.near.at[0, 1], self.nxt, self.n)
+            send(self.view(at(self.me, -1), 0), self.near.at[1, 0], self.prv, self.n)
 
         def mid(self):
             for h, d, to in ((0, 1, self.nxt), (1, -1, self.prv)):
                 self.f[h].wait_recv()
                 v = self.view(at(self.me, d), h)
                 v[...] = add(v[...], self.far[h]).astype(BF)
-                self.n.append(send(v, self.near.at[h, h], to))
+                send(v, self.near.at[h, h], to, self.n)
 
         def result(self):
-            wait_recv(self.n)
+            self.n.wait_recv()
             for h in range(2):
                 v = self.view(self.me, h)
                 yield h, add(v[...], self.near[0, h]) + self.near[1, h].astype(F32)
@@ -201,23 +221,21 @@
             t2, got, raw = self.t2, self.got, self.raw
             for h, v in self.y1.result():
                 t2[h] = v.astype(BF)
-            self.c1 = [
-                send(t2.at[xl, r], got.at[0], xn),
-                send(t2.at[xl, 1 - r], got.at[1], xp),
-            ]
-            self.c2 = [
-                send(t2.at[ox, 1 - mine], raw.at[0], xn),
-                send(t2.at[ox, 1 - mine], raw.at[1], xp),
-            ]
+            self.c1, self.c2 = Group(), Group()
+            send(t2.at[xl, r], got.at[0], xn, self.c1)
+            send(t2.at[xl, 1 - r], got.at[1], xp, self.c1)
+            send(t2.at[ox, 1 - mine], raw.at[0], xn, self.c2)
+            send(t2.at[ox, 1 - mine], raw.at[1], xp, self.c2)
 
         def second_x_mid(self):
-            wait_recv(self.c1)
+            self.c1.wait_recv()
             v = self.t2.at[ox, mine]
             v[...] = (add(self.got[0], self.got[1]) + v[...].astype(F32)).astype(BF)
-            self.c2 += [send(v, self.vb.at[0], xn), send(v, self.vb.at[1], xp)]
+            send(v, self.vb.at[0], xn, self.c2)
+            send(v, self.vb.at[1], xp, self.c2)
 
         def store_second(self, out):
-            wait_recv(self.c2)
+            self.c2.wait_recv()
             out[1, 1 - r] = add(self.vb[0], self.raw[1]) * norm
             out[1, r] = add(self.vb[1], self.raw[0]) * norm
 
@@ -242,32 +260,36 @@
             same(rows_of(wd, y, xl, 512 * h, 512), to)
             for h, to in ((0, yn), (1, yp), (1, yn), (0, yp))
         ]
-        wdx = {d: [] for d in (0, 1, -1, 2)}
-        wdx[0] = [x_send(wd, 0, 512, y, h) for h in range(2)]
+        wdx = {d: Group() for d in (0, 1, -1, 2)}
+        for h in range(2):
+            x_send(wd, 0, 512, y, h, wdx[0])
         pre1 = send(pre, pre_r, dev(core=oc))
         wu_x = [x_send(wu, 64, 32, y, h) for h in range(2)]
     with scope("b_wd_first"):
         wd1[0].wait_recv()
         wd2 = [same(rows_of(wd, at(y, -1), xl, 0, 512), yn)]
-        wdx[-1].append(x_send(wd, 0, 512, at(y, -1), 0))
+        x_send(wd, 0, 512, at(y, -1), 0, wdx[-1])
         wd1[1].wait_recv()
         wd2.append(same(rows_of(wd, at(y, 1), xl, 512, 512), yp))
-        wdx[1].append(x_send(wd, 0, 512, at(y, 1), 1))
+        x_send(wd, 0, 512, at(y, 1), 1, wdx[1])
     with scope("c_z_forward"):
         s2 = z_forward(xs, s1)
         a1 = z_send(loc_a, xa)
     with scope("d_wd_second"):
         wd1[2].wait_recv()
-        wdx[-1].append(x_send(wd, 0, 512, at(y, -1), 1))
+        x_send(wd, 0, 512, at(y, -1), 1, wdx[-1])
         wd1[3].wait_recv()
-        wdx[1].append(x_send(wd, 0, 512, at(y, 1), 0))
+        x_send(wd, 0, 512, at(y, 1), 0, wdx[1])
         wuy = [same(rows_of(wu, y, xl, 0, 64), to) for to in (yn, yp)]
-        wuo = [same(rows_of(wu, y, xl, 64, 64), to) for to in (yn, yp)]
+        wux = Group()
+        wuo = same(rows_of(wu, y, xl, 64, 64), yn)
+        same(rows_of(wu, y, xl, 64, 64), yp, wux)
         wuo2 = []
         for h in range(2):
             wu_x[h].wait_recv()
             piece = rows_of(wu, y, ox, 64 + 32 * h, 32)
-            wuo2 += [same(piece, yn), same(piece, yp)]
+            same(piece, yn, wux)
+            wuo2.append(same(piece, yp))
     with scope("e_act"):
         act_t[:, 0:256] = relu_sq(pre[...]).T
         pre1.wait_recv()
@@ -275,10 +297,11 @@
     with scope("f_wd_third"):
         for h in range(2):
             wd2[h].wait_recv()
-            wdx[2].append(x_send(wd, 0, 512, at(y, 2), h))
-        wux = [x_send(wu, 0, 32, y, h) for h in range(2)]
+            x_send(wd, 0, 512, at(y, 2), h, wdx[2])
+        for h in range(2):
+            x_send(wu, 0, 32, y, h, wux)
     with scope("g_scaled_wait"):
-        wait_recv(s2)
+        s2.wait_recv()
     with scope("h_grad_down"):
         for k in range(4):
             part = nn(act_t[...], xs[k])
@@ -293,13 +316,14 @@
             wuy[h].wait_recv()
             k = at(y, d)
             wuf.append(same(rows_of(wu, k, xl, 32 * h, 32), to))
-            wux += [x_send(wu, 0, 32, k, 0), x_send(wu, 0, 32, k, 1)]
+            x_send(wu, 0, 32, k, 0, wux)
+            x_send(wu, 0, 32, k, 1, wux)
     with scope("j_acts_forward"):
         a2 = z_forward(xa, a1)
     dax = []
     for d in (0, 1, -1, 2):
         with scope("k_wd_wait"):
-            wait_recv(wdx[d])
+            wdx[d].wait_recv()
         with scope("l_d_act"):
             k = at(y, d)
             w = jnp.concatenate([wd[k, 0], wd[k, 1]], axis=1)
@@ -309,11 +333,11 @@
                 if d == 2:
                     dax.append(send(da.at[h], dr.at[1 - h], dev(core=oc)))
     with scope("m_wu_third"):
-        wuo[0].wait_recv()
-        wug = [same(rows_of(wu, at(y, -1), xl, 64, 64), yn)]
-        for h in range(2):
-            wuo2[2 * h + 1].wait_recv()
-            wug.append(same(rows_of(wu, at(y, 1), ox, 64 + 32 * h, 32), yp))
+        wuo.wait_recv()
+        same(rows_of(wu, at(y, -1), xl, 64, 64), yn, wux)
+        for h in range(2):
+            wuo2[h].wait_recv()
+            same(rows_of(wu, at(y, 1), ox, 64 + 32 * h, 32), yp, wux)
         gd.y1.start_near()
     with scope("n_dpre"):
         for h in (1, 0):
@@ -322,7 +346,7 @@
             pos = jnp.maximum(src[...].astype(F32), 0.0)
             dpre[h * 256:(h + 1) * 256, :] = (2.0 * pos * (da[h] + dr[h]) * ups[...]).astype(BF)
     with scope("o_acts_wait"):
-        wait_recv(a2)
+        a2.wait_recv()
     with scope("p_grad_up"):
         for k in range(4):
             part = nn(xa[k].T, dpre[...])
@@ -331,14 +355,13 @@
     with scope("q_gd_mid"):
         for h in range(2):
             wuf[h].wait_recv()
-            wux.append(x_send(wu, 0, 32, at(y, 2), h))
+            x_send(wu, 0, 32, at(y, 2), h, wux)
         gd.x1.mid()
         gd.y1.mid()
         gu.start()
     zr = Ring(lambda k, h: gi.at[k, pl.ds(256 * h, 256), :], z, farz, nearz, zn, zp)
     with scope("r_wu_wait"):
-        wait_recv(wux)
-        wait_recv(wuo[1:] + [wuo2[0], wuo2[2]] + wug)
+        wux.wait_recv()
     with scope("s_grad_in"):
         for d in (2, 1, -1, 0):
             k = at(z, d)
@@ -357,11 +380,12 @@
     with scope("w_gd_second_mid"):
         gd.y2.mid()
         gd.second_x_mid()
+    with scope("x_gu_second_x"):
+        gu.second_x()
+    with scope("x_gu_second_y"):
+        gu.second_y()
     with scope("y_gd_share"):
         gd.share()
-    with scope("x_gu_second"):
-        gu.second_y()
-        gu.second_x()
     with scope("z_gi"):
         for h, v in zr.result():
             fz[h] = v.astype(BF)
@@ -387,8 +411,8 @@
     with scope("zg_gu_out"):
         gu.store_first(gu_out)
     with scope("zh_drain"):
-        for copy in started:
-            copy.wait_send()
+        assert recvs[0] == RECVS and sum(started) == SENT_ROWS, (recvs, sum(started))
+        pltpu.make_async_copy(sent, sent, ssem).wait()
 
 
 def body(acts, cotangent, pre_act, up_store, up_scale, down_store, down_scale):
@@ -414,9 +438,9 @@
         call,
         name="ffn_backward",
         out_shape=(
-            jax.ShapeDtypeStruct((256, 512), BF),
-            jax.ShapeDtypeStruct((2, 2, 32, 1024), F32),
-            jax.ShapeDtypeStruct((2, 2, 256, 128), F32),
+            pltpu.VMEM((256, 512), BF),
+            pltpu.VMEM((2, 2, 32, 1024), F32),
+            pltpu.VMEM((2, 2, 256, 128), F32),
         ),
         in_specs=[pl.BlockSpec(memory_space=pl.ANY)] * 7,
         out_specs=(spec,) * 3,
@@ -429,8 +453,9 @@
             vm(4, 512, 256), vm(2, 256, 256), vm(2, 2, 256, 256), vm(2, 256, 256), vm(256, 256),
             vm(256, 512), vm(256, 512), vm(256, 1024), vm(128, 1024, dtype=F32),
             vm(1, 1024, dtype=F32), vm(1024, 128, dtype=F32), vm(1, 2048, dtype=F32),
-            pltpu.SemaphoreType.DMA((COPIES,)),
-            pltpu.SemaphoreType.DMA((COPIES,)),
+            vm(SENT_ROWS, 128),
+            pltpu.SemaphoreType.DMA,
+            pltpu.SemaphoreType.DMA((RECVS,)),
             pltpu.SemaphoreType.DMA((7,)),
         ],
         compiler_params=pltpu.CompilerParams(

time: 68 us -> 63 us (0.926)
  Pallas kernels: 63.3 us -> 59.9 us
  local copies, waits for them, and re-layouts: 3.75 us -> 2.29 us
    pallas_call x1, Pallas kernels: 63.3 us -> 59.9 us  [body(): pl.pallas_call(call, name='ffn_backward', out_shape=(pltpu.VMEM((256, 512...]
    unnamed x7 -> x3, local copies, waits for them, and re-layouts: 3.75 us -> 2.29 us
where the time goes in v4:
time: 63 us; the launch traced here: 62.9 us
  Pallas kernels  59.9 us (95%)
  local copies, waits for them, and re-layouts  2.29 us (4%)
  between operations  0.64 us (1%)
    pallas_call x1, Pallas kernels, body(): pl.pallas_call(call, name='ffn_backward', out_shape=(pltpu.VMEM((256, 512...  59.9 us
    unnamed x3, local copies, waits for them, and re-layouts  2.29 us

profile of v4, /device:TPU:0, one launch (start us, length us, event | category | flops | bytes accessed | tf_op | source)
XLA Modules:
  0.0 62.9 jit_solution(10782071515767802053)
XLA Ops:
  0.6 59.9 %ffn_backward.1 = (bf16[256,512]{1,0:T(8,128)(2,1)S(1)}, f32[2,2,32,1024]{3,2,1,0:T(8,128)S(1)}, f32[2,2,256,128]{3,2,1,0:T(8,128)S(1)}) custom-call(bf16[256,512]{1,0:T(8,128)(2,1)} %args_0_.4, bf16[256,512]{1,0:T(8,128)(2,1)} %args_1_.4, bf16[256,1024]{1,0:T(8,128)(2,1)} %args_2_.4, f32[128,1024]{1,0:T(8,128)} %args_3_.4, f32[1,1024]{1,0:T(1,128)} %bitcast.7, ...), custom_call_target="tpu_custom_call" | custom-call | tf_op jit(solution)/shard_map/ffn_backward/pallas_call | solution.py:437
  60.6 0.7 %copy.13 = bf16[256,512]{1,0:T(8,128)(2,1)} copy(bf16[256,512]{1,0:T(8,128)(2,1)S(1)} %get-tuple-element.9) | data formatting | bytes 524288
  61.3 0.8 %copy.14 = f32[128,1024]{1,0:T(8,128)} copy(f32[128,1024]{1,0:T(8,128)S(1)} %bitcast.5) | data formatting | bytes 1048576
  62.1 0.8 %copy.15 = f32[1024,128]{1,0:T(8,128)} copy(f32[1024,128]{1,0:T(8,128)S(1)} %bitcast.4) | data formatting | bytes 1048576

commit v5 on v4

--- a/solution.py
+++ b/solution.py
@@ -11,6 +11,7 @@
 F32 = jnp.float32
 MESH = pl.DeviceIdType.MESH
 RECVS = 57
+Y_FIRST = 64
 SENT_ROWS = 52736
 
 
@@ -264,7 +265,12 @@
         for h in range(2):
             x_send(wd, 0, 512, y, h, wdx[0])
         pre1 = send(pre, pre_r, dev(core=oc))
-        wu_x = [x_send(wu, 64, 32, y, h) for h in range(2)]
+        ya, yh = Y_FIRST, Y_FIRST // 2
+        xr, xh = 128 - ya, (128 - ya) // 2
+        wu_x = [x_send(wu, ya, xh, y, h) for h in range(2)]
+        wux = Group()
+        for h in range(2):
+            x_send(wu, 0, yh, y, h, wux)
     with scope("b_wd_first"):
         wd1[0].wait_recv()
         wd2 = [same(rows_of(wd, at(y, -1), xl, 0, 512), yn)]
@@ -280,14 +286,13 @@
         x_send(wd, 0, 512, at(y, -1), 1, wdx[-1])
         wd1[3].wait_recv()
         x_send(wd, 0, 512, at(y, 1), 0, wdx[1])
-        wuy = [same(rows_of(wu, y, xl, 0, 64), to) for to in (yn, yp)]
-        wux = Group()
-        wuo = same(rows_of(wu, y, xl, 64, 64), yn)
-        same(rows_of(wu, y, xl, 64, 64), yp, wux)
+        wuy = [same(rows_of(wu, y, xl, 0, ya), to) for to in (yn, yp)]
+        wuo = same(rows_of(wu, y, xl, ya, xr), yn)
+        same(rows_of(wu, y, xl, ya, xr), yp, wux)
         wuo2 = []
         for h in range(2):
             wu_x[h].wait_recv()
-            piece = rows_of(wu, y, ox, 64 + 32 * h, 32)
+            piece = rows_of(wu, y, ox, ya + xh * h, xh)
             same(piece, yn, wux)
             wuo2.append(same(piece, yp))
     with scope("e_act"):
@@ -298,8 +303,6 @@
         for h in range(2):
             wd2[h].wait_recv()
             x_send(wd, 0, 512, at(y, 2), h, wdx[2])
-        for h in range(2):
-            x_send(wu, 0, 32, y, h, wux)
     with scope("g_scaled_wait"):
         s2.wait_recv()
     with scope("h_grad_down"):
@@ -315,9 +318,9 @@
         for h, to, d in ((0, yn, -1), (1, yp, 1)):
             wuy[h].wait_recv()
             k = at(y, d)
-            wuf.append(same(rows_of(wu, k, xl, 32 * h, 32), to))
-            x_send(wu, 0, 32, k, 0, wux)
-            x_send(wu, 0, 32, k, 1, wux)
+            wuf.append(same(rows_of(wu, k, xl, yh * h, yh), to))
+            x_send(wu, 0, yh, k, 0, wux)
+            x_send(wu, 0, yh, k, 1, wux)
     with scope("j_acts_forward"):
         a2 = z_forward(xa, a1)
     dax = []
@@ -334,10 +337,10 @@
                     dax.append(send(da.at[h], dr.at[1 - h], dev(core=oc)))
     with scope("m_wu_third"):
         wuo.wait_recv()
-        same(rows_of(wu, at(y, -1), xl, 64, 64), yn, wux)
+        same(rows_of(wu, at(y, -1), xl, ya, xr), yn, wux)
         for h in range(2):
             wuo2[h].wait_recv()
-            same(rows_of(wu, at(y, 1), ox, 64 + 32 * h, 32), yp, wux)
+            same(rows_of(wu, at(y, 1), ox, ya + xh * h, xh), yp, wux)
         gd.y1.start_near()
     with scope("n_dpre"):
         for h in (1, 0):
@@ -355,7 +358,7 @@
     with scope("q_gd_mid"):
         for h in range(2):
             wuf[h].wait_recv()
-            x_send(wu, 0, 32, at(y, 2), h, wux)
+            x_send(wu, 0, yh, at(y, 2), h, wux)
         gd.x1.mid()
         gd.y1.mid()
         gu.start()
@@ -370,23 +373,24 @@
                 zr.start_far()
             if d == -1:
                 zr.start_near()
+    with scope("u_gu_x1_mid"):
+        gu.x1.mid()
+    with scope("u_z_mid"):
+        zr.mid()
+    with scope("u_gu_y1_mid"):
+        gu.y1.mid()
     with scope("t_gd_second"):
         gd.second_y()
         gd.second_x()
-    with scope("u_gu_mid"):
-        gu.mid()
-    with scope("v_z_mid"):
-        zr.mid()
-    with scope("w_gd_second_mid"):
+    with scope("w_gu_second_y"):
+        gu.second_y()
+    with scope("v_gd_x2_mid"):
+        gd.second_x_mid()
+    with scope("y_gu_second_x"):
+        gu.second_x()
+    with scope("v_gd_y2_mid"):
         gd.y2.mid()
-        gd.second_x_mid()
-    with scope("x_gu_second_x"):
-        gu.second_x()
-    with scope("x_gu_second_y"):
-        gu.second_y()
-    with scope("y_gd_share"):
-        gd.share()
-    with scope("z_gi"):
+    with scope("x_gi"):
         for h, v in zr.result():
             fz[h] = v.astype(BF)
         gx = send(fz.at[1], rz, dev(core=oc))
@@ -394,6 +398,10 @@
         gu.y2.mid()
     with scope("zb_gu_x2_mid"):
         gu.second_x_mid()
+    with scope("zd_gu_share"):
+        gu.share()
+    with scope("z_gd_share"):
+        gd.share()
     with scope("zc_gi_out"):
         gx.wait_recv()
         for j in range(2):
@@ -401,8 +409,6 @@
             gi_out[:, lanes] = fz[0, :, j * 128:(j + 1) * 128]
             lanes = pl.ds(pl.multiple_of(j * 256 + oc * 128, 128), 128)
             gi_out[:, lanes] = rz[:, j * 128:(j + 1) * 128]
-    with scope("zd_gu_share"):
-        gu.share()
     with scope("ze_gd_out"):
         gd.store_first(gd_out)
         gd.store_second(gd_out)
@@ -413,6 +419,17 @@
     with scope("zh_drain"):
         assert recvs[0] == RECVS and sum(started) == SENT_ROWS, (recvs, sum(started))
         pltpu.make_async_copy(sent, sent, ssem).wait()
+
+
+def write_out(a, b, c, x, y, z, sems):
+    copies = [
+        pltpu.make_async_copy(v, w, sems.at[i])
+        for i, (v, w) in enumerate(((a, x), (b, y), (c, z)))
+    ]
+    for k in copies:
+        k.start()
+    for k in copies:
+        k.wait()
 
 
 def body(acts, cotangent, pre_act, up_store, up_scale, down_store, down_scale):
@@ -465,6 +482,15 @@
         cotangent, acts, pre_act, up_store, up_scale.reshape(1, -1),
         down_store, down_scale.reshape(1, -1),
     )
+    outs = [pltpu.with_memory_space_constraint(v, pltpu.VMEM) for v in (gi, gu, gd)]
+    gi, gu, gd = pl.pallas_call(
+        write_out,
+        name="write_out",
+        out_shape=tuple(jax.ShapeDtypeStruct(v.shape, v.dtype) for v in outs),
+        in_specs=[spec] * 3,
+        out_specs=(pl.BlockSpec(memory_space=pl.ANY),) * 3,
+        scratch_shapes=[pltpu.SemaphoreType.DMA((3,))],
+    )(*outs)
     return gi, gu.reshape(up_store.shape), gd.reshape(down_store.shape)
 
 

time: 63 us -> 60.1 us (0.954)
  local copies, waits for them, and re-layouts: 2.29 us -> 0 us
    unnamed x3 -> x0, local copies, waits for them, and re-layouts: 2.29 us -> none
    pallas_call x1, Pallas kernels: 59.9 us -> 58.2 us  [body(): pl.pallas_call(call, name='ffn_backward', out_shape=(pltpu.VMEM((256, 512...]
    pallas_call x0 -> x1, Pallas kernels: none -> 1.08 us  [body(): pl.pallas_call(write_out, name='write_out', out_shape=tuple((jax.ShapeDty...]
where the time goes in v5:
time: 60.1 us; the launch traced here: 59.9 us
  Pallas kernels  59.3 us (99%)
  between operations  0.64 us (1%)
    pallas_call x1, Pallas kernels, body(): pl.pallas_call(call, name='ffn_backward', out_shape=(pltpu.VMEM((256, 512...  58.2 us

profile of v5, /device:TPU:0, one launch (start us, length us, event | category | flops | bytes accessed | tf_op | source)
XLA Modules:
  0.0 59.9 jit_solution(14536769369266793382)
XLA Ops:
  0.6 58.2 %ffn_backward.1 = (bf16[256,512]{1,0:T(8,128)(2,1)S(1)}, f32[2,2,32,1024]{3,2,1,0:T(8,128)S(1)}, f32[2,2,256,128]{3,2,1,0:T(8,128)S(1)}) custom-call(bf16[256,512]{1,0:T(8,128)(2,1)} %args_0_.4, bf16[256,512]{1,0:T(8,128)(2,1)} %args_1_.4, bf16[256,1024]{1,0:T(8,128)(2,1)} %args_2_.4, f32[128,1024]{1,0:T(8,128)} %args_3_.4, f32[1,1024]{1,0:T(1,128)} %bitcast.5, ...), custom_call_target="tpu_custom_call" | custom-call | tf_op jit(solution)/shard_map/ffn_backward/pallas_call | solution.py:454
  58.8 1.1 %write_out.1 = (bf16[256,512]{1,0:T(8,128)(2,1)}, f32[2,2,32,1024]{3,2,1,0:T(8,128)}, f32[2,2,256,128]{3,2,1,0:T(8,128)}) custom-call(bf16[256,512]{1,0:T(8,128)(2,1)S(1)} %get-tuple-element.9.a, f32[2,2,32,1024]{3,2,1,0:T(8,128)S(1)} %get-tuple-element.10.b, f32[2,2,256,128]{3,2,1,0:T(8,128)S(1)} %get-tuple-element.11.c), custom_call_target="tpu_custom_call" | custom-call | tf_op jit(solution)/shard_map/write_out/pallas_call | solution.py:486

commit v6 on v5

--- a/solution.py
+++ b/solution.py
@@ -10,7 +10,7 @@
 BF = jnp.bfloat16
 F32 = jnp.float32
 MESH = pl.DeviceIdType.MESH
-RECVS = 57
+RECVS = 69
 Y_FIRST = 64
 SENT_ROWS = 52736
 
@@ -28,7 +28,8 @@
     gi_out, gu_out, gd_out,
     loc_s, loc_a, xs, xa, pre_r, act_t, wd, wu, da, dr, dpre,
     pd, td1, td2, fd, rd, farxd, nearxd, gotd, rawd, vd, faryd, nearyd, faryd2, nearyd2,
-    pu, tu1, tu2, fu, ru, farxu, nearxu, gotu, rawu, vu, faryu, nearyu, faryu2, nearyu2,
+    pua, tu1a, tu2a, fua, rua, farxua, nearxua, gotua, rawua, vua, faryua, nearyua, faryu2a, nearyu2a,
+    pub, tu1b, tu2b, fub, rub, farxub, nearxub, gotub, rawub, vub, faryub, nearyub, faryu2b, nearyu2b,
     gi, farz, nearz, fz, rz,
     cot, acts, pre, up, ups, down, dsc,
     sent, ssem, rsem, lsem,
@@ -60,8 +61,8 @@
 
     loads = {}
     for i, (n, src, dst) in enumerate((
-        ("dsc", dsc_h, dsc), ("cot", cot_h, cot), ("down", down_h, down), ("acts", acts_h, acts),
-        ("up", up_h, up), ("pre", pre_h, pre), ("ups", ups_h, ups),
+        ("down", down_h, down), ("dsc", dsc_h, dsc), ("cot", cot_h, cot), ("up", up_h, up),
+        ("pre", pre_h, pre), ("acts", acts_h, acts), ("ups", ups_h, ups),
     )):
         loads[n] = pltpu.make_async_copy(src, dst, lsem.at[i])
         loads[n].start()
@@ -101,20 +102,8 @@
                 lanes = slice(j * 256 + k * 128, j * 256 + k * 128 + 128)
                 dst[k, :, j * 128:(j + 1) * 128] = v[:, lanes]
 
-    loads["dsc"].wait()
-    scale = dsc[:, pl.ds(pl.multiple_of(z * 512, 512), 512)]
-    loads["cot"].wait()
-    split(loc_s, (cot[...].astype(F32) * scale).astype(BF))
-    xs[z, 0:256, :] = loc_s[c]
     loads["down"].wait()
     wd[y, xl] = down[...].astype(BF)
-    loads["acts"].wait()
-    split(loc_a, acts[...])
-    xa[z, 0:256, :] = loc_a[c]
-    loads["up"].wait()
-    wu[y, xl] = up[...].astype(BF)
-    loads["pre"].wait()
-    loads["ups"].wait()
     pl.semaphore_wait(barrier, len(peers))
 
     own, other = pl.ds(0, 256), pl.ds(256, 256)
@@ -252,11 +241,11 @@
 
     mine = r * xl + (1 - r) * ox
     gd = Grad(pd, td1, td2, fd, rd, farxd, nearxd, gotd, rawd, vd, faryd, nearyd, faryd2, nearyd2)
-    gu = Grad(pu, tu1, tu2, fu, ru, farxu, nearxu, gotu, rawu, vu, faryu, nearyu, faryu2, nearyu2)
+    ga = Grad(pua, tu1a, tu2a, fua, rua, farxua, nearxua, gotua, rawua, vua, faryua, nearyua, faryu2a, nearyu2a)
+    gb = Grad(pub, tu1b, tu2b, fub, rub, farxub, nearxub, gotub, rawub, vub, faryub, nearyub, faryu2b, nearyu2b)
     scope = jax.named_scope
 
     with scope("a_first_sends"):
-        s1 = z_send(loc_s, xs)
         wd1 = [
             same(rows_of(wd, y, xl, 512 * h, 512), to)
             for h, to in ((0, yn), (1, yp), (1, yn), (0, yp))
@@ -264,13 +253,26 @@
         wdx = {d: Group() for d in (0, 1, -1, 2)}
         for h in range(2):
             x_send(wd, 0, 512, y, h, wdx[0])
-        pre1 = send(pre, pre_r, dev(core=oc))
+        loads["dsc"].wait()
+        scale = dsc[:, pl.ds(pl.multiple_of(z * 512, 512), 512)]
+        loads["cot"].wait()
+        split(loc_s, (cot[...].astype(F32) * scale).astype(BF))
+        s1 = z_send(loc_s, xs)
+        xs[z, 0:256, :] = loc_s[c]
+        loads["up"].wait()
+        wu[y, xl] = up[...].astype(BF)
         ya, yh = Y_FIRST, Y_FIRST // 2
         xr, xh = 128 - ya, (128 - ya) // 2
         wu_x = [x_send(wu, ya, xh, y, h) for h in range(2)]
         wux = Group()
         for h in range(2):
             x_send(wu, 0, yh, y, h, wux)
+        loads["pre"].wait()
+        pre1 = send(pre, pre_r, dev(core=oc))
+        loads["acts"].wait()
+        split(loc_a, acts[...])
+        xa[z, 0:256, :] = loc_a[c]
+        loads["ups"].wait()
     with scope("b_wd_first"):
         wd1[0].wait_recv()
         wd2 = [same(rows_of(wd, at(y, -1), xl, 0, 512), yn)]
@@ -351,17 +353,21 @@
     with scope("o_acts_wait"):
         a2.wait_recv()
     with scope("p_grad_up"):
-        for k in range(4):
-            part = nn(xa[k].T, dpre[...])
-            for j in range(2):
-                pu[k, j] = part[j * 128:(j + 1) * 128, :].astype(BF).reshape(2, 2, 32, 1024)
+        for i, g in enumerate((ga, gb)):
+            cols = slice(i * 512, i * 512 + 512)
+            for k in range(4):
+                part = nn(xa[k].T, dpre[:, cols])
+                for j in range(2):
+                    g.p[k, j] = part[j * 128:(j + 1) * 128, :].astype(BF).reshape(2, 2, 32, 512)
     with scope("q_gd_mid"):
         for h in range(2):
             wuf[h].wait_recv()
             x_send(wu, 0, yh, at(y, 2), h, wux)
         gd.x1.mid()
         gd.y1.mid()
-        gu.start()
+        ga.start()
+        gb.y1.start_far()
+        gb.x1.start_far()
     zr = Ring(lambda k, h: gi.at[k, pl.ds(256 * h, 256), :], z, farz, nearz, zn, zp)
     with scope("r_wu_wait"):
         wux.wait_recv()
@@ -373,35 +379,54 @@
                 zr.start_far()
             if d == -1:
                 zr.start_near()
-    with scope("u_gu_x1_mid"):
-        gu.x1.mid()
+    with scope("ga_x1"):
+        ga.x1.mid()
+    with scope("ga_y1"):
+        ga.y1.mid()
+    with scope("gb_nx"):
+        gb.x1.start_near()
+    with scope("gb_ny"):
+        gb.y1.start_near()
+    with scope("gb_x1"):
+        gb.x1.mid()
     with scope("u_z_mid"):
         zr.mid()
-    with scope("u_gu_y1_mid"):
-        gu.y1.mid()
-    with scope("t_gd_second"):
+    with scope("gb_y1"):
+        gb.y1.mid()
+    with scope("t_y"):
         gd.second_y()
+    with scope("t_x"):
         gd.second_x()
-    with scope("w_gu_second_y"):
-        gu.second_y()
+    with scope("ga_sy"):
+        ga.second_y()
+    with scope("ga_sx"):
+        ga.second_x()
+    with scope("w_gb_second_y"):
+        gb.second_y()
+    with scope("w_gb_second_x"):
+        gb.second_x()
     with scope("v_gd_x2_mid"):
         gd.second_x_mid()
-    with scope("y_gu_second_x"):
-        gu.second_x()
     with scope("v_gd_y2_mid"):
         gd.y2.mid()
+    with scope("ga_ym"):
+        ga.y2.mid()
+    with scope("ga_xm"):
+        ga.second_x_mid()
+    with scope("y_gb_y2_mid"):
+        gb.y2.mid()
+    with scope("z_gd_share"):
+        gd.share()
+    with scope("z_ga_share"):
+        ga.share()
+    with scope("y_gb_x2_mid"):
+        gb.second_x_mid()
+    with scope("z_gb_share"):
+        gb.share()
     with scope("x_gi"):
         for h, v in zr.result():
             fz[h] = v.astype(BF)
         gx = send(fz.at[1], rz, dev(core=oc))
-    with scope("za_gu_y2_mid"):
-        gu.y2.mid()
-    with scope("zb_gu_x2_mid"):
-        gu.second_x_mid()
-    with scope("zd_gu_share"):
-        gu.share()
-    with scope("z_gd_share"):
-        gd.share()
     with scope("zc_gi_out"):
         gx.wait_recv()
         for j in range(2):
@@ -409,13 +434,13 @@
             gi_out[:, lanes] = fz[0, :, j * 128:(j + 1) * 128]
             lanes = pl.ds(pl.multiple_of(j * 256 + oc * 128, 128), 128)
             gi_out[:, lanes] = rz[:, j * 128:(j + 1) * 128]
-    with scope("ze_gd_out"):
-        gd.store_first(gd_out)
-        gd.store_second(gd_out)
-    with scope("zf_gu_out"):
-        gu.store_second(gu_out)
-    with scope("zg_gu_out"):
-        gu.store_first(gu_out)
+    outs = [(gd, gd_out)] + [(g, gu_out.at[:, :, :, pl.ds(i * 512, 512)]) for i, g in ((0, ga), (1, gb))]
+    with scope("ze_second_out"):
+        for g, out in outs:
+            g.store_second(out)
+    with scope("zf_first_out"):
+        for g, out in outs:
+            g.store_first(out)
     with scope("zh_drain"):
         assert recvs[0] == RECVS and sum(started) == SENT_ROWS, (recvs, sum(started))
         pltpu.make_async_copy(sent, sent, ssem).wait()
@@ -466,7 +491,8 @@
             vm(256, 1024), vm(1024, 512), vm(4, 2, 1024, 128), vm(4, 2, 128, 1024),
             vm(2, 256, 1024, dtype=F32), vm(2, 256, 1024, dtype=F32), vm(512, 1024),
             *grad_bufs(256, 128),
-            *grad_bufs(32, 1024),
+            *grad_bufs(32, 512),
+            *grad_bufs(32, 512),
             vm(4, 512, 256), vm(2, 256, 256), vm(2, 2, 256, 256), vm(2, 256, 256), vm(256, 256),
             vm(256, 512), vm(256, 512), vm(256, 1024), vm(128, 1024, dtype=F32),
             vm(1, 1024, dtype=F32), vm(1024, 128, dtype=F32), vm(1, 2048, dtype=F32),

time: 60.1 us -> 59.8 us (level)
  no operation moved by 1% of the time
where the time goes in v6:
time: 59.8 us; the launch traced here: 59.7 us
  Pallas kernels  59 us (99%)
  between operations  0.64 us (1%)
    pallas_call x1, Pallas kernels, body(): pl.pallas_call(call, name='ffn_backward', out_shape=(pltpu.VMEM((256, 512...  57.9 us

profile of v6, /device:TPU:0, one launch (start us, length us, event | category | flops | bytes accessed | tf_op | source)
XLA Modules:
  0.0 59.7 jit_solution(17547353270441498260)
XLA Ops:
  0.6 57.9 %ffn_backward.1 = (bf16[256,512]{1,0:T(8,128)(2,1)S(1)}, f32[2,2,32,1024]{3,2,1,0:T(8,128)S(1)}, f32[2,2,256,128]{3,2,1,0:T(8,128)S(1)}) custom-call(bf16[256,512]{1,0:T(8,128)(2,1)} %args_0_.4, bf16[256,512]{1,0:T(8,128)(2,1)} %args_1_.4, bf16[256,1024]{1,0:T(8,128)(2,1)} %args_2_.4, f32[128,1024]{1,0:T(8,128)} %args_3_.4, f32[1,1024]{1,0:T(1,128)} %bitcast.5, ...), custom_call_target="tpu_custom_call" | custom-call | tf_op jit(solution)/shard_map/ffn_backward/pallas_call | solution.py:479
  58.6 1.1 %write_out.1 = (bf16[256,512]{1,0:T(8,128)(2,1)}, f32[2,2,32,1024]{3,2,1,0:T(8,128)}, f32[2,2,256,128]{3,2,1,0:T(8,128)}) custom-call(bf16[256,512]{1,0:T(8,128)(2,1)S(1)} %get-tuple-element.9.a, f32[2,2,32,1024]{3,2,1,0:T(8,128)S(1)} %get-tuple-element.10.b, f32[2,2,256,128]{3,2,1,0:T(8,128)S(1)} %get-tuple-element.11.c), custom_call_target="tpu_custom_call" | custom-call | tf_op jit(solution)/shard_map/write_out/pallas_call | solution.py:512

commit v7 on v6

--- a/solution.py
+++ b/solution.py
@@ -312,7 +312,6 @@
             part = nn(act_t[...], xs[k])
             for j in range(2):
                 pd[k, j] = part[:, j * 128:(j + 1) * 128].astype(BF).reshape(2, 2, 256, 128)
-        gd.y1.start_far()
         gd.x1.start_far()
         gd.x1.start_near()
     with scope("i_wu_second"):
@@ -323,6 +322,7 @@
             wuf.append(same(rows_of(wu, k, xl, yh * h, yh), to))
             x_send(wu, 0, yh, k, 0, wux)
             x_send(wu, 0, yh, k, 1, wux)
+        gd.y1.start_far()
     with scope("j_acts_forward"):
         a2 = z_forward(xa, a1)
     dax = []
@@ -344,6 +344,11 @@
             wuo2[h].wait_recv()
             same(rows_of(wu, at(y, 1), ox, ya + xh * h, xh), yp, wux)
         gd.y1.start_near()
+    with scope("m_x_sends"):
+        for h in range(2):
+            wuf[h].wait_recv()
+            x_send(wu, 0, yh, at(y, 2), h, wux)
+        gd.x1.mid()
     with scope("n_dpre"):
         for h in (1, 0):
             dax[1 - h].wait_recv()
@@ -360,10 +365,6 @@
                 for j in range(2):
                     g.p[k, j] = part[j * 128:(j + 1) * 128, :].astype(BF).reshape(2, 2, 32, 512)
     with scope("q_gd_mid"):
-        for h in range(2):
-            wuf[h].wait_recv()
-            x_send(wu, 0, yh, at(y, 2), h, wux)
-        gd.x1.mid()
         gd.y1.mid()
         ga.start()
         gb.y1.start_far()

time: 59.8 us -> 59.8 us (level)
  no operation moved by 1% of the time
where the time goes in v7:
time: 59.8 us; the launch traced here: 59.7 us
  Pallas kernels  59 us (99%)
  between operations  0.64 us (1%)
    pallas_call x1, Pallas kernels, body(): pl.pallas_call(call, name='ffn_backward', out_shape=(pltpu.VMEM((256, 512...  57.9 us

profile of v7, /device:TPU:0, one launch (start us, length us, event | category | flops | bytes accessed | tf_op | source)
XLA Modules:
  0.0 59.7 jit_solution(1499860296186623388)
XLA Ops:
  0.6 57.9 %ffn_backward.1 = (bf16[256,512]{1,0:T(8,128)(2,1)S(1)}, f32[2,2,32,1024]{3,2,1,0:T(8,128)S(1)}, f32[2,2,256,128]{3,2,1,0:T(8,128)S(1)}) custom-call(bf16[256,512]{1,0:T(8,128)(2,1)} %args_0_.4, bf16[256,512]{1,0:T(8,128)(2,1)} %args_1_.4, bf16[256,1024]{1,0:T(8,128)(2,1)} %args_2_.4, f32[128,1024]{1,0:T(8,128)} %args_3_.4, f32[1,1024]{1,0:T(1,128)} %bitcast.5, ...), custom_call_target="tpu_custom_call" | custom-call | tf_op jit(solution)/shard_map/ffn_backward/pallas_call | solution.py:480
  58.6 1.1 %write_out.1 = (bf16[256,512]{1,0:T(8,128)(2,1)}, f32[2,2,32,1024]{3,2,1,0:T(8,128)}, f32[2,2,256,128]{3,2,1,0:T(8,128)}) custom-call(bf16[256,512]{1,0:T(8,128)(2,1)S(1)} %get-tuple-element.9.a, f32[2,2,32,1024]{3,2,1,0:T(8,128)S(1)} %get-tuple-element.10.b, f32[2,2,256,128]{3,2,1,0:T(8,128)S(1)} %get-tuple-element.11.c), custom_call_target="tpu_custom_call" | custom-call | tf_op jit(solution)/shard_map/write_out/pallas_call | solution.py:513
